TPU v7x, 512 devices: a whole 4x4x16 slice. The times are simulated.
512 devices in a mesh: kv: 64 (over z, y), tp: 8 (over x, core).
Axes of the slice: x: 4, y: 4, z: 16, core: 2. Of those that a mesh axis runs over, the one named last changes fastest.
Arguments:
- stream: bfloat16 [32, 4096], P(None, 'kv'), may hold values from -32 to 32
- gain_in: bfloat16 [4096], P('kv'), may hold values from 0.099609375 to 1.8984375
- w_query: bfloat16 [4096, 2048], P('kv', 'tp'), may hold values from -0.09375 to 0.09375
- w_key: bfloat16 [4096, 2048], P('kv', 'tp'), may hold values from -0.09375 to 0.09375
- w_value: bfloat16 [4096, 2048], P('kv', 'tp'), may hold values from -0.09375 to 0.09375
- w_forget: bfloat16 [4096, 16], replicated, may hold values from -0.09375 to 0.09375
- keys_cache: bfloat16 [32, 16, 8192, 128], P(None, 'tp', 'kv'), may hold values from -136 to 136
- values_cache: bfloat16 [32, 16, 8192, 128], P(None, 'tp', 'kv'), may hold values from -6 to 6
- decay_cache: float32 [32, 16, 8192], P(None, 'tp', 'kv'), may hold values from -1283 to 0
- lengths: int32 [32], replicated, may hold values from 1 to 8192, 104889 in all
- gain_att: bfloat16 [2048], P('tp'), may hold values from 0.099609375 to 1.8984375
- w_out: bfloat16 [2048, 4096], P('tp', 'kv'), may hold values from -0.125 to 0.125
- gain_mlp: bfloat16 [4096], P('kv'), may hold values from 0.099609375 to 1.8984375
- w_up: bfloat16 [4096, 16384], P('kv', 'tp'), may hold values from -0.09375 to 0.09375
- w_down: bfloat16 [16384, 4096], P('tp', 'kv'), may hold values from -0.046875 to 0.046875
Outputs:
- updated: bfloat16 [32, 4096], P(None, 'kv')
Inputs may be any that keep to these rules, and one draw needn't show every extreme that they name: `lengths`: one sequence has all 8192 positions live.
All inputs are finite; a program needn't handle non-finite values.
Results may differ from a plain program's by a relative error of at most 0.012.
The roundings to bfloat16 on the way count: a program that leaves them out, or rounds other values in their place, can miss the bound.
Values may be sent and summed in bfloat16 or wider, within the bound.
A program may use at most 64 MiB of HBM per device.

v0:
```python
import math

import jax
import jax.numpy as jnp
from jax import lax
from jax.sharding import Mesh
from jax.sharding import PartitionSpec as P

KV = ("kv_0", "kv_1")


norm_eps = 1e-06
masked_score = -1e30


def padded_to(lines, devices):
    spare = -lines.shape[0] % devices
    if not spare:
        return lines
    return jnp.concatenate([lines, jnp.zeros((spare, *lines.shape[1:]), lines.dtype)])


def laid_out(parts, dim):
    parts = jnp.moveaxis(parts, 0, dim)
    lengths = parts.shape
    return parts.reshape(*lengths[:dim], lengths[dim] * lengths[dim + 1], *lengths[dim + 2 :])


def sent_to_all(value, axis):
    copies = jnp.broadcast_to(value, (lax.axis_size(axis), *value.shape))
    return lax.all_to_all(copies, axis, split_axis=0, concat_axis=0, tiled=True)


def gather_directly(value, axis, dim):
    return laid_out(sent_to_all(value, axis), dim)


def cut_along(value, dim, devices):
    lengths = value.shape
    parts = value.reshape(*lengths[:dim], devices, lengths[dim] // devices, *lengths[dim + 1 :])
    return jnp.moveaxis(parts, dim, 0)


def sum_at_owner(value, axis, dim):
    devices = lax.axis_size(axis)
    parts = lax.all_to_all(cut_along(value, dim, devices), axis, 0, 0, tiled=True)
    return jnp.sum(parts, axis=0)


def sum_by_parts(value, axes):
    padded = padded_to(value, lax.axis_size(axes))
    whole = gather_directly(sum_at_owner(padded, axes, 0), axes, 0)
    return lax.slice_in_dim(whole, 0, len(value)).reshape(value.shape)


def together(arrays, axis):
    line, at, finished = (jnp.concatenate([a.reshape(-1) for a in arrays]), 0, [])
    so_far = sum_by_parts(line, axis)
    for a in arrays:
        finished.append(so_far[at : at + a.size].reshape(a.shape))
        at += a.size
    return tuple(finished)


def all_in_one(value, axis):
    leaves = jax.tree.leaves(value)
    turns = sorted(range(len(leaves)), key=lambda k: -leaves[k].size)
    width = (1, *leaves[turns[0]].shape)[-1]
    lines = [
        jnp.pad(leaves[k].reshape(-1), (0, -leaves[k].size % width)).reshape(-1, width)
        for k in turns
    ]
    both, at, found = (lax.all_gather(jnp.concatenate(lines), axis), 0, {})
    for k, line in zip(turns, lines):
        share = both[:, at : at + len(line)].reshape(len(both), -1)
        found[k] = share[:, : leaves[k].size].reshape(-1, *leaves[k].shape)
        at += len(line)
    numbers = iter(range(len(leaves)))
    return jax.tree.map(lambda _: found[next(numbers)], value)


def joined_all(value, axes, combine):
    for axis in axes:
        pieces = all_in_one(value, axis)
        value = jax.tree.map(lambda part: part[0], pieces)
        for k in range(1, lax.axis_size(axis)):
            value = combine(value, jax.tree.map(lambda part: part[k], pieces))
    return value


def over_copies(value, axis):
    everything = sent_to_all(value, axis)
    return jnp.sum(everything, axis=0)


def fold_parts(left_part, right_part):
    peak_all = jnp.maximum(left_part[0], right_part[0])
    weight_one = jnp.exp(left_part[0] - peak_all)
    weight_two = jnp.exp(right_part[0] - peak_all)
    total_sum = left_part[1] * weight_one + right_part[1] * weight_two
    merged = left_part[2] * weight_one[..., None] + right_part[2] * weight_two[..., None]
    return (peak_all, total_sum, merged)


def per_device(
    stream,
    gain_in,
    w_query,
    w_key,
    w_value,
    w_forget,
    keys_cache,
    values_cache,
    decay_cache,
    lengths,
    gain_att,
    w_out,
    gain_mlp,
    w_up,
    w_down,
):
    kv_index = lax.axis_index(KV)
    tp_index = lax.axis_index("tp")
    kv_count = lax.axis_size(KV)
    seqs_here, cols_here = stream.shape
    heads_here = keys_cache.shape[1]
    pos_here = keys_cache.shape[2]
    head_dim = keys_cache.shape[3]
    width_all = cols_here * kv_count
    score_scale = 1.0 / math.sqrt(head_dim)
    stream_float = stream.astype(jnp.float32)
    scaled = (stream_float * gain_in.astype(jnp.float32)).astype(jnp.bfloat16)
    square_sum = jnp.sum(stream_float * stream_float, axis=1)
    forget_rows = lax.dynamic_slice(
        w_forget, (kv_index * cols_here, tp_index * heads_here), (cols_here, heads_here)
    )
    part_query = jnp.dot(scaled, w_query, preferred_element_type=jnp.float32)
    part_key = jnp.dot(scaled, w_key, preferred_element_type=jnp.float32)
    part_value = jnp.dot(scaled, w_value, preferred_element_type=jnp.float32)
    part_forget = jnp.dot(scaled, forget_rows, preferred_element_type=jnp.float32)
    part_query, part_key, part_value, part_forget, square_total = together(
        (part_query, part_key, part_value, part_forget, square_sum), KV
    )
    scale_in = lax.rsqrt(square_total / width_all + norm_eps)[:, None]
    queries = (part_query * scale_in).astype(jnp.bfloat16).reshape(seqs_here, heads_here, head_dim)
    key_new = (part_key * scale_in).astype(jnp.bfloat16).reshape(seqs_here, heads_here, head_dim)
    value_new = (
        (part_value * scale_in).astype(jnp.bfloat16).reshape(seqs_here, heads_here, head_dim)
    )
    forget = jax.nn.log_sigmoid(part_forget * scale_in)
    attention_logits = (
        jnp.einsum("shd,shpd->shp", queries, keys_cache, preferred_element_type=jnp.float32)
        * score_scale
    )
    attention_logits = attention_logits + forget[:, :, None] + decay_cache
    cache_positions = kv_index * pos_here + lax.iota(jnp.int32, pos_here)
    live_mask = (cache_positions[None, :] < lengths[:, None])[:, None, :]
    attention_logits = jnp.where(live_mask, attention_logits, masked_score)
    block_peak = jnp.max(attention_logits, axis=2)
    weights = jnp.where(live_mask, jnp.exp(attention_logits - block_peak[..., None]), 0.0)
    block_total = jnp.sum(weights, axis=2)
    block_out = jnp.einsum(
        "shp,shpd->shd",
        weights.astype(jnp.bfloat16),
        values_cache,
        preferred_element_type=jnp.float32,
    )
    peak_all, total_all, out_all = joined_all((block_peak, block_total, block_out), KV, fold_parts)
    own_score = (
        jnp.sum(queries.astype(jnp.float32) * key_new.astype(jnp.float32), axis=2) * score_scale
    )
    top_score = jnp.maximum(peak_all, own_score)
    past_weight = jnp.exp(peak_all - top_score)
    own_weight = jnp.exp(own_score - top_score)
    numerator = (
        out_all * past_weight[..., None] + value_new.astype(jnp.float32) * own_weight[..., None]
    )
    denominator = total_all * past_weight + own_weight
    attended = (numerator / denominator[..., None]).reshape(seqs_here, heads_here * head_dim)
    attended_in = (attended * gain_att.astype(jnp.float32)).astype(jnp.bfloat16)
    part_out = jnp.dot(attended_in, w_out, preferred_element_type=jnp.float32)
    att_squares = jnp.sum(attended * attended, axis=1)
    part_out, att_total = (over_copies(part_out, "tp"), over_copies(att_squares, "tp"))
    scale_att = lax.rsqrt(att_total / (attended.shape[1] * lax.axis_size("tp")) + norm_eps)[:, None]
    residual = (stream_float + scale_att * part_out).astype(jnp.bfloat16)
    residual_float = residual.astype(jnp.float32)
    mixer_in = (residual_float * gain_mlp.astype(jnp.float32)).astype(jnp.bfloat16)
    mixer_squares = jnp.sum(residual_float * residual_float, axis=1)
    part_up = jnp.dot(mixer_in, w_up, preferred_element_type=jnp.float32)
    square_cols = jnp.broadcast_to(mixer_squares[:, None], (seqs_here, kv_count))
    share_units, share_total = (sum_at_owner(part_up, KV, 1), sum_at_owner(square_cols, KV, 1))
    scale_mixer = lax.rsqrt(share_total / width_all + norm_eps)
    hidden_share = jnp.square(jax.nn.relu(share_units * scale_mixer)).astype(jnp.bfloat16)
    hidden = gather_directly(hidden_share, KV, 1)
    part_down = jnp.dot(hidden, w_down, preferred_element_type=jnp.float32)
    mixer_out = over_copies(part_down, "tp")
    return (residual_float + mixer_out).astype(jnp.bfloat16)


def solution(mesh):
    split = Mesh(mesh.devices.reshape(16, 4, mesh.shape["tp"]), ("kv_0", "kv_1", "tp"))
    return jax.shard_map(
        per_device,
        mesh=split,
        in_specs=(
            P(None, KV),
            P(KV),
            P(KV, "tp"),
            P(KV, "tp"),
            P(KV, "tp"),
            P(),
            P(None, "tp", KV, None),
            P(None, "tp", KV, None),
            P(None, "tp", KV),
            P(),
            P("tp"),
            P("tp", KV),
            P(KV),
            P(KV, "tp"),
            P("tp", KV),
        ),
        out_specs=P(None, KV),
        check_vma=False,
    )
```

profile of v0, /device:TPU:1, one launch (start us, length us, event | category | flops | bytes accessed | tf_op | source)
XLA Modules:
  0.0 224.7 jit_solution(15841474211591573087)
XLA Ops:
  0.0 0.8 convert_element_type.75
  0.8 0.8 fusion.60
  1.6 0.9 fusion.72
  2.6 0.9 convolution_bitcast_fusion.2
  3.5 0.9 convolution_bitcast_fusion.1
  4.5 0.9 convolution_bitcast_fusion
  5.8 34.1 %all_to_all.46 = f32[64,1,386]{2,1,0:T(1,128)S(1)} all-to-all(f32[64,1,386]{2,1,0:T(1,128)S(1)} %all_to_all.29), channel_id=1, replica_groups=mesh['kv_0'=16,'kv_1'=4,'tp'=8] {'kv_0','kv_1'}, dimensions={0} | all-to-all | bytes 197632 | tf_op jit(solution)/shard_map/all_to_all | solution.py:46
  40.7 6.3 %all-to-all-start.1 = ((f32[64,1,386]{2,1,0:T(1,128)}), f32[64,1,386]{2,1,0:T(1,128)S(1)}, u32[]{:S(2)}, u32[]{:S(2)}) async-start(f32[64,1,386]{2,1,0:T(1,128)} %broadcast_in_dim.32), calls=%async_computation.1 | async-start | bytes 262144 | tf_op jit(solution)/shard_map/all_to_all | solution.py:31
  48.3 0.7 broadcast_compare_fusion
  49.0 13.0 %all-to-all-done.1 = f32[64,1,386]{2,1,0:T(1,128)S(1)} async-done(((f32[64,1,386]{2,1,0:T(1,128)}), f32[64,1,386]{2,1,0:T(1,128)S(1)}, u32[]{:S(2)}, u32[]{:S(2)}) %all-to-all-start.1) | async-done | bytes 98848 | tf_op jit(solution)/shard_map/all_to_all | solution.py:31
  62.7 3.5 %slice.349 = f32[12352,2]{1,0:T(8,128)} reshape(f32[64,386]{1,0:T(8,128)S(1)} %reduce.6) | data formatting | bytes 197632 | tf_op jit(solution)/shard_map/slice | solution.py:60
  66.4 0.8 fusion.65
  67.4 1.2 fusion.56
  69.2 2.2 fusion.54
  71.5 22.8 %all-gather.2 = f32[16,66,128]{2,1,0:T(8,128)S(1)} all-gather(f32[1,66,128]{2,1,0:T(8,128)S(1)} %maximum_bitcast_fusion), channel_id=2, replica_groups=mesh['kv_0'=16,'kv_1'=4,'tp'=8] {'kv_0'}, dimensions={0}, use_global_device_ids=true | all-gather | bytes 574464 | tf_op jit(solution)/shard_map/all_gather | solution.py:73
  94.8 9.4 %all-gather.3 = f32[4,66,128]{2,1,0:T(8,128)S(1)} all-gather(f32[1,66,128]{2,1,0:T(8,128)S(1)} %maximum_bitcast_fusion.1), channel_id=3, replica_groups=mesh['kv_0'=16,'kv_1'=4,'tp'=8] {'kv_1'}, dimensions={0}, use_global_device_ids=true | all-gather | bytes 168960 | tf_op jit(solution)/shard_map/all_gather | solution.py:73
  108.3 17.4 %all-to-all-start.2 = ((f32[8,1,32]{2,1,0:T(1,128)}), f32[8,1,32]{2,1,0:T(1,128)S(1)}, u32[]{:S(2)}, u32[]{:S(2)}) async-start(f32[8,1,32]{2,1,0:T(1,128)} %broadcast_in_dim.35), calls=%async_computation.2 | async-start | bytes 8192 | tf_op jit(solution)/shard_map/all_to_all | solution.py:31
  126.8 0.7 reshape.1676
  127.6 2.6 %all-to-all-done.2 = f32[8,1,32]{2,1,0:T(1,128)S(1)} async-done(((f32[8,1,32]{2,1,0:T(1,128)}), f32[8,1,32]{2,1,0:T(1,128)S(1)}, u32[]{:S(2)}, u32[]{:S(2)}) %all-to-all-start.2) | async-done | bytes 1056 | tf_op jit(solution)/shard_map/all_to_all | solution.py:31
  130.2 3.9 %all-to-all-start.3 = ((f32[8,1,2048]{2,1,0:T(1,128)}), f32[8,1,2048]{2,1,0:T(1,128)S(1)}, u32[]{:S(2)}, u32[]{:S(2)}) async-start(f32[8,1,2048]{2,1,0:T(1,128)} %reshape.1676), calls=%async_computation.3 | async-start | bytes 131072 | tf_op jit(solution)/shard_map/all_to_all | solution.py:31
  134.2 4.8 %all-to-all-done.3 = f32[8,1,2048]{2,1,0:T(1,128)S(1)} async-done(((f32[8,1,2048]{2,1,0:T(1,128)}), f32[8,1,2048]{2,1,0:T(1,128)S(1)}, u32[]{:S(2)}, u32[]{:S(2)}) %all-to-all-start.3) | async-done | bytes 65568 | tf_op jit(solution)/shard_map/all_to_all | solution.py:31
  139.5 0.8 reduce.41
  141.3 6.8 %all-to-all-start.5 = ((f32[64,32,1]{1,2,0:T(1,128)}), f32[64,32,1]{1,2,0:T(1,128)S(1)}, u32[]{:S(2)}, u32[]{:S(2)}) async-start(f32[64,32,1]{1,2,0:T(1,128)} %transpose.61), calls=%async_computation.5 | async-start | bytes 65536 | tf_op jit(solution)/shard_map/all_to_all | solution.py:46
  148.6 1.6 copy.98
  150.2 2.4 %reshape.1678 = f32[64,1,1024]{2,1,0:T(1,128)} reshape(f32[64,32,32]{2,1,0:T(8,128)} %copy.98) | data formatting | bytes 524288
  152.6 9.0 %all-to-all-done.5 = f32[64,32,1]{1,2,0:T(1,128)S(1)} async-done(((f32[64,32,1]{1,2,0:T(1,128)}), f32[64,32,1]{1,2,0:T(1,128)S(1)}, u32[]{:S(2)}, u32[]{:S(2)}) %all-to-all-start.5) | async-done | bytes 8224 | tf_op jit(solution)/shard_map/all_to_all | solution.py:46
  161.6 5.7 %all-to-all-start.4 = ((f32[64,1,1024]{2,1,0:T(1,128)}), f32[64,1,1024]{2,1,0:T(1,128)S(1)}, u32[]{:S(2)}, u32[]{:S(2)}) async-start(f32[64,1,1024]{2,1,0:T(1,128)} %reshape.1678), calls=%async_computation.4 | async-start | bytes 524288 | tf_op jit(solution)/shard_map/all_to_all | solution.py:46
  167.4 18.8 %all-to-all-done.4 = f32[64,1,1024]{2,1,0:T(1,128)S(1)} async-done(((f32[64,1,1024]{2,1,0:T(1,128)}), f32[64,1,1024]{2,1,0:T(1,128)S(1)}, u32[]{:S(2)}, u32[]{:S(2)}) %all-to-all-start.4) | async-done | bytes 262176 | tf_op jit(solution)/shard_map/all_to_all | solution.py:46
  186.2 1.3 reduce.42
  188.4 22.5 %all_to_all.47 = bf16[64,2,512]{2,1,0:T(2,128)(2,1)S(1)} all-to-all(bf16[64,2,512]{2,1,0:T(2,128)(2,1)S(1)} %reshape.1680), channel_id=1, replica_groups=mesh['kv_0'=16,'kv_1'=4,'tp'=8] {'kv_0','kv_1'}, dimensions={0} | all-to-all | bytes 262144 | tf_op jit(solution)/shard_map/all_to_all | solution.py:31
  212.4 10.8 %all_to_all.48 = f32[8,1,2048]{2,1,0:T(1,128)S(1)} all-to-all(f32[8,1,2048]{2,1,0:T(1,128)S(1)} %reshape.1682), channel_id=1, replica_groups=mesh['kv_0'=16,'kv_1'=4,'tp'=8] {'tp'}, dimensions={0} | all-to-all | bytes 131072 | tf_op jit(solution)/shard_map/all_to_all | solution.py:31
  223.2 0.8 reduce.43
  (124 shorter events, 14.8 us)
Async XLA Ops:
  0.0 67.4 %copy-start = (bf16[32,2,128,128]{3,2,1,0:T(8,128)(2,1)S(1)}, bf16[32,2,128,128]{3,2,1,0:T(8,128)(2,1)}, u32[]{:S(2)}) copy-start(bf16[32,2,128,128]{3,2,1,0:T(8,128)(2,1)} %param.21) | copy-start | bytes 6291460
  40.7 21.3 %all-to-all-start.1 = ((f32[64,1,386]{2,1,0:T(1,128)}), f32[64,1,386]{2,1,0:T(1,128)S(1)}, u32[]{:S(2)}, u32[]{:S(2)}) async-start(f32[64,1,386]{2,1,0:T(1,128)} %broadcast_in_dim.32), calls=%async_computation.1 | async-start | bytes 262144 | tf_op jit(solution)/shard_map/all_to_all | solution.py:31
  66.2 2.4 %copy-start.5 = (f32[32,2,128]{2,1,0:T(2,128)S(1)}, f32[32,2,128]{2,1,0:T(2,128)}, u32[]{:S(2)}) copy-start(f32[32,2,128]{2,1,0:T(2,128)} %param.23) | copy-start | bytes 98308
  71.5 55.1 %copy-start.4 = (bf16[256,64]{0,1:T(8,128)(2,1)S(1)}, bf16[256,64]{0,1:T(8,128)(2,1)}, u32[]{:S(2)}) copy-start(bf16[256,64]{0,1:T(8,128)(2,1)} %param.26) | copy-start | bytes 98308
  94.4 46.1 %copy-start.1 = (bf16[32,64]{1,0:T(8,128)(2,1)S(1)}, bf16[32,64]{1,0:T(8,128)(2,1)}, u32[]{:S(2)}) copy-start(bf16[32,64]{1,0:T(8,128)(2,1)} %param.15) | copy-start | bytes 12292
  94.5 53.6 %copy-start.2 = (bf16[64,2048]{1,0:T(8,128)(2,1)S(1)}, bf16[64,2048]{1,0:T(8,128)(2,1)}, u32[]{:S(2)}) copy-start(bf16[64,2048]{1,0:T(8,128)(2,1)} %param.28) | copy-start | bytes 786436
  108.3 21.9 %all-to-all-start.2 = ((f32[8,1,32]{2,1,0:T(1,128)}), f32[8,1,32]{2,1,0:T(1,128)S(1)}, u32[]{:S(2)}, u32[]{:S(2)}) async-start(f32[8,1,32]{2,1,0:T(1,128)} %broadcast_in_dim.35), calls=%async_computation.2 | async-start | bytes 8192 | tf_op jit(solution)/shard_map/all_to_all | solution.py:31
  130.2 8.8 %all-to-all-start.3 = ((f32[8,1,2048]{2,1,0:T(1,128)}), f32[8,1,2048]{2,1,0:T(1,128)S(1)}, u32[]{:S(2)}, u32[]{:S(2)}) async-start(f32[8,1,2048]{2,1,0:T(1,128)} %reshape.1676), calls=%async_computation.3 | async-start | bytes 131072 | tf_op jit(solution)/shard_map/all_to_all | solution.py:31
  141.3 20.3 %all-to-all-start.5 = ((f32[64,32,1]{1,2,0:T(1,128)}), f32[64,32,1]{1,2,0:T(1,128)S(1)}, u32[]{:S(2)}, u32[]{:S(2)}) async-start(f32[64,32,1]{1,2,0:T(1,128)} %transpose.61), calls=%async_computation.5 | async-start | bytes 65536 | tf_op jit(solution)/shard_map/all_to_all | solution.py:46
  161.6 24.5 %all-to-all-start.4 = ((f32[64,1,1024]{2,1,0:T(1,128)}), f32[64,1,1024]{2,1,0:T(1,128)S(1)}, u32[]{:S(2)}, u32[]{:S(2)}) async-start(f32[64,1,1024]{2,1,0:T(1,128)} %reshape.1678), calls=%async_computation.4 | async-start | bytes 524288 | tf_op jit(solution)/shard_map/all_to_all | solution.py:46
  187.9 24.1 %copy-start.3 = (bf16[2048,64]{0,1:T(8,128)(2,1)S(1)}, bf16[2048,64]{0,1:T(8,128)(2,1)}, u32[]{:S(2)}) copy-start(bf16[2048,64]{0,1:T(8,128)(2,1)} %param.29) | copy-start | bytes 786436
where the time goes:
time: 226 us; the launch traced here: 225 us
  blocking collectives  99.7 us (44%)
  waiting for transfers between devices  48.3 us (21%)
  starting transfers between devices  40 us (18%)
  local copies, waits for them, and re-layouts  18.2 us (8%)
  other arithmetic  10.4 us (5%)
  matrix products  7.55 us (3%)
    all_to_all x1, blocking collectives, sum_at_owner(): lax.all_to_all(cut_along(value, dim, devices), axis, 0, 0, tiled=True)  34.1 us
    all_to_all x2, blocking collectives, sent_to_all(): return lax.all_to_all(copies, axis, split_axis=0, concat_axis=0, tiled=True)  33.3 us
    all_gather x2, blocking collectives, all_in_one(): both, at, found = (lax.all_gather(jnp.concatenate(lines), axis), 0, {})  32.3 us
    all_to_all x2, waiting for transfers between devices, sum_at_owner(): lax.all_to_all(cut_along(value, dim, devices), axis, 0, 0, tiled=True)  27.8 us
    all_to_all x3, starting transfers between devices, sent_to_all(): return lax.all_to_all(copies, axis, split_axis=0, concat_axis=0, tiled=True)  27.6 us
    all_to_all x3, waiting for transfers between devices, sent_to_all(): return lax.all_to_all(copies, axis, split_axis=0, concat_axis=0, tiled=True)  20.5 us
    all_to_all x2, starting transfers between devices, sum_at_owner(): lax.all_to_all(cut_along(value, dim, devices), axis, 0, 0, tiled=True)  12.4 us
    unnamed x24, local copies, waits for them, and re-layouts  4.64 us
  transfers between devices with their start and end apart: 5, of which 5 were waited for; matrix products, arithmetic and copies ran while one was open for 4% of the time, Pallas kernels for 0%

commit v1 on v0

v1 whole, which is shorter than its diff:
```python
import math

import jax
import jax.numpy as jnp
from jax import lax
from jax.experimental import pallas as pl
from jax.experimental.pallas import tpu as pltpu
from jax.sharding import PartitionSpec as P

f32, bf16 = jnp.float32, jnp.bfloat16
MESH = pl.DeviceIdType.MESH
NORM_EPS = 1e-06
MASKED = -1e30

NZ, NY, NTP = 16, 4, 8
NKV = NZ * NY
SEQS, HEADS, HD, POS = 32, 2, 128, 128
COLS, UNITS = 64, 2048
D, HW = NKV * COLS, NTP * HEADS * HD
BLOCKS = UNITS // 128

QKV, QUERY, PART, ATT, OUT, UP, SQUARES, HIDDEN, DOWN = range(9)
EXCHANGES = 9


def kernel(
    stream_ref, gain_in_ref, wq_hbm, wk_hbm, wv_hbm, wf_hbm, keys_hbm, values_hbm, decay_ref,
    lengths_ref, gain_att_ref, wo_hbm, gain_mlp_ref, wu_hbm, wd_hbm,
    out_ref,
    wq, wk, wv, wf, keys, values, wo, wu, wd,
    len_buf, score_buf, prob_buf,
    send1, recv1, send_q, recv_q, send2, recv2, send_a, recv_a, send_o, recv_o,
    send_u, recv_u, send_s, recv_s, send_h, recv_h, send_d, recv_d,
    load_sem, send_sem, recv_sem,
):
    kv, tp = lax.axis_index("kv"), lax.axis_index("tp")
    z, y = kv // NY, lax.rem(kv, NY)

    def kv_peer(i):
        ring = i // NY
        dz = NZ // 2 + (1 - 2 * lax.rem(ring, 2)) * ((ring + 1) // 2)
        dy = i + i // (NKV - NY)
        return lax.rem(z + dz, NZ) * NY + lax.rem(y + dy, NY)

    def tp_peer(i):
        return lax.rem(tp + 1 + i, NTP)

    barrier = pltpu.get_barrier_semaphore()

    def greet_kv(i, c):
        pl.semaphore_signal(barrier, 1, device_id=(kv_peer(i), tp), device_id_type=MESH)
        return c

    def greet_tp(i, c):
        pl.semaphore_signal(barrier, 1, device_id=(kv, tp_peer(i)), device_id_type=MESH)
        return c

    lax.fori_loop(0, NKV - 1, greet_kv, 0)
    lax.fori_loop(0, NTP - 1, greet_tp, 0)

    rows = pl.ds(pl.multiple_of(kv * COLS, COLS), COLS)
    loads = [
        (wq_hbm, wq), (wk_hbm, wk), (wv_hbm, wv), (wf_hbm.at[rows, :], wf),
        (keys_hbm, keys), (values_hbm, values), (wo_hbm, wo), (wu_hbm, wu), (wd_hbm, wd),
    ]
    loads = [pltpu.make_async_copy(a, b, load_sem.at[k]) for k, (a, b) in enumerate(loads)]
    for load in loads:
        load.start()

    lane = lax.broadcasted_iota(jnp.int32, (SEQS, 128), 1)
    low_half = lane < 64

    def to_kv(name, source, target):
        def step(i, c):
            peer = kv_peer(i)
            pltpu.make_async_remote_copy(
                src_ref=source(peer), dst_ref=target, send_sem=send_sem.at[name],
                recv_sem=recv_sem.at[name], device_id=(peer, tp), device_id_type=MESH,
            ).start()
            return c

        lax.fori_loop(0, NKV - 1, step, 0)

    def to_tp(name, source, target):
        def step(i, c):
            pltpu.make_async_remote_copy(
                src_ref=source, dst_ref=target, send_sem=send_sem.at[name],
                recv_sem=recv_sem.at[name], device_id=(kv, tp_peer(i)), device_id_type=MESH,
            ).start()
            return c

        lax.fori_loop(0, NTP - 1, step, 0)

    def arrived(name, buffer):
        n = buffer.shape[0] - 1
        whole = buffer.at[pl.ds(0, n)]
        pltpu.make_async_copy(whole, whole, recv_sem.at[name]).wait()

    def sent(name, buffer):
        n = buffer.shape[0] - 1
        whole = buffer.at[pl.ds(0, n)]
        pltpu.make_async_copy(whole, whole, send_sem.at[name]).wait()

    stream = stream_ref[...].astype(f32)
    scaled = (stream * gain_in_ref[...].astype(f32)).astype(bf16)
    squares = jnp.sum(stream * stream, axis=1, keepdims=True)
    for s in range(SEQS):
        len_buf[s : s + 1, :] = jnp.full((1, 128), lengths_ref[s], jnp.int32)
    for k in range(4):
        loads[k].wait()
    part_f = jnp.dot(scaled, wf[...], preferred_element_type=f32)
    lane_f = lax.broadcasted_iota(jnp.int32, part_f.shape, 1)
    for r, w in enumerate((wq, wk, wv)):
        part = jnp.dot(scaled, w[...], preferred_element_type=f32)
        for h in range(HEADS):
            send1[h * SEQS : (h + 1) * SEQS, r, :] = part[:, h * HD : (h + 1) * HD]
    for h in range(HEADS):
        gate = jnp.sum(jnp.where(lane_f == tp * HEADS + h, part_f, 0.0), axis=1, keepdims=True)
        send1[h * SEQS : (h + 1) * SEQS, 3, :] = jnp.where(low_half, gate, squares)
    recv1[kv] = send1[kv]
    pl.semaphore_wait(barrier, NKV - 1 + NTP - 1)
    to_kv(QKV, lambda peer: send1.at[peer], recv1.at[kv])
    arrived(QKV, recv1)
    total = jnp.sum(recv1[...], axis=0)
    extra = total[3:4, :]
    lane_1 = lax.broadcasted_iota(jnp.int32, (1, 128), 1)
    gate_sum = jnp.sum(jnp.where(lane_1 == 0, extra, 0.0), axis=1, keepdims=True)
    square_sum = jnp.sum(jnp.where(lane_1 == 127, extra, 0.0), axis=1, keepdims=True)
    scale_in = lax.rsqrt(square_sum / D + NORM_EPS)
    query = (total[0:1, :] * scale_in).astype(bf16).astype(f32)
    send_q[...] = query
    recv_q[kv] = query
    to_kv(QUERY, lambda peer: send_q, recv_q.at[kv])
    key_new = (total[1:2, :] * scale_in).astype(bf16).astype(f32)
    value_new = (total[2:3, :] * scale_in).astype(bf16).astype(f32)
    gate_in = gate_sum * scale_in
    forget = jnp.minimum(gate_in, 0.0) - jnp.log1p(jnp.exp(-jnp.abs(gate_in)))
    score_scale = 1.0 / math.sqrt(HD)
    own = jnp.sum(query * key_new, axis=1, keepdims=True) * score_scale

    loads[4].wait()
    arrived(QUERY, recv_q)

    def score_rows(k, c):
        for h in range(HEADS):
            rows = []
            for j in range(8):
                q = recv_q[h * SEQS + k * 8 + j].astype(bf16)
                rows.append(
                    lax.dot_general(
                        q, keys[k * 8 + j, h], (((1,), (1,)), ((), ())), preferred_element_type=f32
                    )
                )
            at = pl.multiple_of(h * SEQS + k * 8, 8)
            score_buf[pl.ds(at, 8), :] = jnp.concatenate(rows, axis=0)
        return c

    lax.fori_loop(0, SEQS // 8, score_rows, 0)
    live = kv * POS + lane < len_buf[...]
    for h in range(HEADS):
        rows = slice(h * SEQS, (h + 1) * SEQS)
        logits = score_buf[rows, :] * score_scale + decay_ref[:, h, :]
        logits = jnp.where(live, logits, MASKED)
        peak = jnp.max(logits, axis=1, keepdims=True)
        probs = jnp.where(live, jnp.exp(logits - peak), 0.0)
        block_total = jnp.sum(probs, axis=1, keepdims=True)
        prob_buf[rows, :] = probs
        send2[rows, 1, :] = jnp.where(low_half, peak, block_total)
    loads[5].wait()

    def value_rows(k, c):
        for h in range(HEADS):
            at = pl.multiple_of(h * SEQS + k * 8, 8)
            probs = prob_buf[pl.ds(at, 8), :]
            for j in range(8):
                row = jnp.dot(
                    probs[j : j + 1, :].astype(bf16), values[k * 8 + j, h],
                    preferred_element_type=f32,
                )
                send2[h * SEQS + k * 8 + j, 0:1, :] = row
        return c

    lax.fori_loop(0, SEQS // 8, value_rows, 0)
    recv2[kv] = send2[kv]
    to_kv(PART, lambda peer: send2.at[peer], recv2.at[kv])
    arrived(PART, recv2)

    block_out, stats = recv2[:, 0, :], recv2[:, 1, :]
    low = lax.broadcasted_iota(jnp.int32, (NKV, 128), 1) < 64
    peaks = jnp.max(jnp.where(low, stats, 2 * MASKED), axis=1, keepdims=True) + forget
    totals = jnp.max(jnp.where(low, 0.0, stats), axis=1, keepdims=True)
    top = jnp.maximum(own, jnp.max(peaks, axis=0, keepdims=True))
    weight = jnp.exp(peaks - top)
    own_weight = jnp.exp(own - top)
    numerator = jnp.sum(weight * block_out, axis=0, keepdims=True) + own_weight * value_new
    denominator = jnp.sum(weight * totals, axis=0, keepdims=True) + own_weight
    attended = numerator / denominator
    send_a[...] = attended
    recv_a[kv] = attended
    to_kv(ATT, lambda peer: send_a, recv_a.at[kv])
    loads[6].wait()
    arrived(ATT, recv_a)

    part_out, att_squares = None, None
    for h in range(HEADS):
        att = recv_a[h * SEQS : (h + 1) * SEQS, 0, :]
        att_in = (att * gain_att_ref[h : h + 1, :].astype(f32)).astype(bf16)
        term = jnp.dot(att_in, wo[h * HD : (h + 1) * HD, :], preferred_element_type=f32)
        square = jnp.sum(att * att, axis=1, keepdims=True)
        part_out = term if h == 0 else part_out + term
        att_squares = square if h == 0 else att_squares + square
    send_o[...] = jnp.concatenate(
        [part_out, jnp.broadcast_to(att_squares, (SEQS, 128 - COLS))], axis=1
    )
    recv_o[tp] = send_o[...]
    to_tp(OUT, send_o, recv_o.at[tp])
    loads[7].wait()
    arrived(OUT, recv_o)
    out_total = jnp.sum(recv_o[...], axis=0)
    scale_att = lax.rsqrt(out_total[:, COLS : COLS + 1] / HW + NORM_EPS)
    residual = (stream + scale_att * out_total[:, :COLS]).astype(bf16).astype(f32)

    mixer_in = (residual * gain_mlp_ref[...].astype(f32)).astype(bf16)
    mixer_squares = jnp.sum(residual * residual, axis=1, keepdims=True)
    row = lax.broadcasted_iota(jnp.int32, (SEQS, 128), 0)
    as_row = jnp.sum(jnp.where(row == lane, mixer_squares, 0.0), axis=0, keepdims=True)
    send_s[...] = as_row
    recv_s[kv] = as_row
    to_kv(SQUARES, lambda peer: send_s, recv_s.at[kv])
    for u in range(BLOCKS):
        part = jnp.dot(mixer_in, wu[:, u * 128 : (u + 1) * 128], preferred_element_type=f32)
        send_u[u * 4 : (u + 1) * 4] = part.astype(bf16).reshape(4, 8, 128)
    recv_u[kv] = send_u[kv]
    to_kv(UP, lambda peer: send_u.at[peer], recv_u.at[kv])
    arrived(SQUARES, recv_s)
    square_row = jnp.sum(recv_s[...], axis=0)
    first = lax.rem(kv, 4) * 8
    pick = lax.broadcasted_iota(jnp.int32, (8, 128), 1) == first + lax.broadcasted_iota(
        jnp.int32, (8, 128), 0
    )
    mixer_total = jnp.sum(jnp.where(pick, square_row, 0.0), axis=1, keepdims=True)
    scale_mixer = lax.rsqrt(mixer_total / D + NORM_EPS)
    arrived(UP, recv_u)
    units = jnp.sum(recv_u[...].astype(f32), axis=0)
    active = jnp.maximum(units * scale_mixer, 0.0)
    hidden = (active * active).astype(bf16)
    send_h[...] = hidden
    recv_h[kv] = hidden
    to_kv(HIDDEN, lambda peer: send_h, recv_h.at[kv])
    loads[8].wait()
    arrived(HIDDEN, recv_h)

    part_down = None
    for u in range(BLOCKS):
        term = jnp.dot(
            recv_h[u * 4 : (u + 1) * 4].reshape(SEQS, 128), wd[u * 128 : (u + 1) * 128, :],
            preferred_element_type=f32,
        )
        part_down = term if u == 0 else part_down + term
    half = SEQS // 2
    send_d[...] = jnp.concatenate([part_down[:half], part_down[half:]], axis=1)
    recv_d[tp] = send_d[...]
    to_tp(DOWN, send_d, recv_d.at[tp])
    arrived(DOWN, recv_d)
    down = jnp.sum(recv_d[...], axis=0)
    down = jnp.concatenate([down[:, :COLS], down[:, COLS:]], axis=0)
    out_ref[...] = (residual + down).astype(bf16)

    for name, buffer in (
        (QKV, recv1), (QUERY, recv_q), (PART, recv2), (ATT, recv_a), (OUT, recv_o),
        (UP, recv_u), (SQUARES, recv_s), (HIDDEN, recv_h), (DOWN, recv_d),
    ):
        sent(name, buffer)


def per_device(
    stream, gain_in, w_query, w_key, w_value, w_forget, keys_cache, values_cache, decay_cache,
    lengths, gain_att, w_out, gain_mlp, w_up, w_down,
):
    vmem = pl.BlockSpec(memory_space=pltpu.VMEM)
    smem = pl.BlockSpec(memory_space=pltpu.SMEM)
    hbm = pl.BlockSpec(memory_space=pl.ANY)
    V = pltpu.VMEM
    scratch = [
        V((COLS, HEADS * HD), bf16), V((COLS, HEADS * HD), bf16), V((COLS, HEADS * HD), bf16),
        V((COLS, 16), bf16),
        V((SEQS, HEADS, POS, HD), bf16), V((SEQS, HEADS, POS, HD), bf16),
        V((HEADS * HD, COLS), bf16), V((COLS, UNITS), bf16), V((UNITS, COLS), bf16),
        V((SEQS, 128), jnp.int32), V((NKV, 128), f32), V((NKV, 128), f32),
        V((NKV, 4, 128), f32), V((NKV, 4, 128), f32),
        V((1, 128), f32), V((NKV, 1, 128), f32),
        V((NKV, 2, 128), f32), V((NKV, 2, 128), f32),
        V((1, 128), f32), V((NKV, 1, 128), f32),
        V((SEQS, 128), f32), V((NTP, SEQS, 128), f32),
        V((NKV, 8, 128), bf16), V((NKV, 8, 128), bf16),
        V((1, 128), f32), V((NKV, 1, 128), f32),
        V((8, 128), bf16), V((NKV, 8, 128), bf16),
        V((SEQS // 2, 128), f32), V((NTP, SEQS // 2, 128), f32),
        pltpu.SemaphoreType.DMA((9,)),
        pltpu.SemaphoreType.DMA((EXCHANGES,)), pltpu.SemaphoreType.DMA((EXCHANGES,)),
    ]
    return pl.pallas_call(
        kernel,
        out_shape=jax.ShapeDtypeStruct((SEQS, COLS), bf16),
        in_specs=[vmem, vmem, hbm, hbm, hbm, hbm, hbm, hbm, vmem, smem, vmem, hbm, vmem, hbm, hbm],
        out_specs=vmem,
        scratch_shapes=scratch,
        compiler_params=pltpu.CompilerParams(collective_id=0, has_side_effects=True),
    )(
        stream, gain_in.reshape(1, COLS), w_query, w_key, w_value, w_forget, keys_cache,
        values_cache, decay_cache, lengths, gain_att.reshape(HEADS, HD), w_out,
        gain_mlp.reshape(1, COLS), w_up, w_down,
    )


def solution(mesh):
    return jax.shard_map(
        per_device,
        mesh=mesh,
        in_specs=(
            P(None, "kv"), P("kv"), P("kv", "tp"), P("kv", "tp"), P("kv", "tp"), P(),
            P(None, "tp", "kv", None), P(None, "tp", "kv", None), P(None, "tp", "kv"), P(),
            P("tp"), P("tp", "kv"), P("kv"), P("kv", "tp"), P("tp", "kv"),
        ),
        out_specs=P(None, "kv"),
        check_vma=False,
    )
```

time: 226 us -> 94.9 us (0.42)
  blocking collectives: 99.7 us -> 0 us
  Pallas kernels: 0 us -> 87.6 us
  waiting for transfers between devices: 48.3 us -> 0 us
  starting transfers between devices: 40 us -> 0 us
  local copies, waits for them, and re-layouts: 18.2 us -> 6.99 us
  other arithmetic: 10.4 us -> 0 us
  matrix products: 7.55 us -> 0 us
    pallas_call x0 -> x1, Pallas kernels: none -> 87.6 us  [per_device(): pl.pallas_call(kernel, out_shape=jax.ShapeDtypeStruct((SEQS, COLS), bf16)...]
    all_to_all x3 -> x0, blocking collectives: 67.5 us -> none  [the longest x1 34.1 us: sum_at_owner(): lax.all_to_all(cut_along(value, dim, devices), axis, 0, 0, tiled=True)]
    all_to_all x5 -> x0, waiting for transfers between devices: 48.3 us -> none  [the longest x2 27.8 us: sum_at_owner(): lax.all_to_all(cut_along(value, dim, devices), axis, 0, 0, tiled=True)]
    all_to_all x5 -> x0, starting transfers between devices: 40 us -> none  [the longest x3 27.6 us: sent_to_all(): return lax.all_to_all(copies, axis, split_axis=0, concat_axis=0, tiled=True)]
    all_gather x2 -> x0, blocking collectives: 32.3 us -> none  [all_in_one(): both, at, found = (lax.all_gather(jnp.concatenate(lines), axis), 0, {})]
    dot_general x9 -> x0, matrix products: 7.55 us -> none  [the longest x1 2.23 us: per_device(): jnp.einsum('shp,shpd->shd', weights.astype(jnp.bfloat16), values_cache, p...]
    slice x6 -> x0, local copies, waits for them, and re-layouts: 3.79 us -> none  [the longest x3 3.75 us: together(): finished.append(so_far[at:at + a.size].reshape(a.shape))]
    all_to_all x4 -> x0, other arithmetic: 3.17 us -> none  [the longest x3 1.91 us: sent_to_all(): return lax.all_to_all(copies, axis, split_axis=0, concat_axis=0, tiled=True)]
  transfers between devices with their start and end apart: 5 -> 0, of which waited for: 5 -> 0; matrix products, arithmetic and copies ran while one was open for 4% -> 0% of each run, Pallas kernels for 0% -> 0%
where the time goes in v1:
time: 94.9 us; the launch traced here: 94.6 us
  Pallas kernels  87.6 us (92%)
  local copies, waits for them, and re-layouts  6.99 us (7%)
    pallas_call x1, Pallas kernels, per_device(): pl.pallas_call(kernel, out_shape=jax.ShapeDtypeStruct((SEQS, COLS), bf16)...  87.6 us
    unnamed x4, local copies, waits for them, and re-layouts  6.99 us

profile of v1, /device:TPU:1, one launch (start us, length us, event | category | flops | bytes accessed | tf_op | source)
XLA Modules:
  0.0 94.6 jit_solution(1205428527158608728)
XLA Ops:
  0.0 1.5 %copy.17.wo_hbm = bf16[256,64]{1,0:T(8,128)(2,1)} copy(bf16[256,64]{0,1:T(8,128)(2,1)} %param.26) | data formatting | bytes 65536 | tf_op args[11]
  1.5 2.0 %copy.18.wd_hbm = bf16[2048,64]{1,0:T(8,128)(2,1)} copy(bf16[2048,64]{0,1:T(8,128)(2,1)} %param.29) | data formatting | bytes 524288 | tf_op args[14]
  3.5 2.2 %copy.16.wf_hbm = bf16[4096,16]{1,0:T(8,128)(2,1)} copy(bf16[4096,16]{0,1:T(8,128)(2,1)} %param.20) | data formatting | bytes 262144 | tf_op args[5]
  5.7 87.6 %shard_map.145 = bf16[32,64]{1,0:T(8,128)(2,1)} custom-call(bf16[32,64]{1,0:T(8,128)(2,1)} %stream_ref.1, bf16[1,64]{1,0:T(2,128)(2,1)} %bitcast.3, bf16[64,256]{1,0:T(8,128)(2,1)} %wq_hbm.1, bf16[64,256]{1,0:T(8,128)(2,1)} %wk_hbm.1, bf16[64,256]{1,0:T(8,128)(2,1)} %wv_hbm.1, bf16[4096,16]{1,0:T(8,128)(2,1)} %copy.16.wf_hbm, ...), custom_call_target="tpu_custom_call" | custom-call | tf_op jit(solution)/shard_map/pallas_call | solution.py:302
  93.3 1.3 %copy.20 = bf16[32,64]{1,0:T(8,128)(2,1)} copy(bf16[32,64]{1,0:T(8,128)(2,1)} %shard_map.145) | data formatting | bytes 8192

commit v2 on v1

v2 whole, which is shorter than its diff:
```python
import math

import jax
import jax.numpy as jnp
from jax import lax
from jax.experimental import pallas as pl
from jax.experimental.pallas import tpu as pltpu
from jax.sharding import PartitionSpec as P

f32, bf16 = jnp.float32, jnp.bfloat16
MESH = pl.DeviceIdType.MESH
NORM_EPS = 1e-06
MASKED = -1e30
NT = (((1,), (1,)), ((), ()))

NZ, NY, NTP = 16, 4, 8
NKV = NZ * NY
SEQS, HEADS, HD, POS = 32, 2, 128, 128
COLS, UNITS = 64, 2048
D, HW = NKV * COLS, NTP * HEADS * HD
BLOCKS = UNITS // 128

QKV, PART, ATT, OUT, OUT_SQ, UP, SQUARES, SCALE, HIDDEN, DOWN = range(10)
EXCHANGES = 10


def kernel(
    stream_hbm, gain_in_hbm, wq_hbm, wk_hbm, wv_hbm, wf_hbm, keys_hbm, values_hbm, decay_hbm,
    lengths_hbm, gain_att_hbm, wo_hbm, gain_mlp_hbm, wu_hbm, wd_hbm,
    out_ref,
    stream_ref, gain_in_ref, wq, wk, wv, wf, keys, values, decay_ref, lengths_ref, gain_att_ref,
    wo, gain_mlp_ref, wu, wd,
    len_buf, bias_buf,
    send1, recv1, send_q, recv_q, send2, recv2, send_a, recv_a, send_o, recv_o, send_os, recv_os,
    send_u, recv_u, send_s, recv_s, recv_t, send_h, recv_h, send_d, recv_d,
    load_sem, send_sem, recv_sem, query_send_sem, query_sem,
):
    kv, tp = lax.axis_index("kv"), lax.axis_index("tp")
    z, y = kv // NY, lax.rem(kv, NY)

    def away(i):
        ring = i // NY
        dz = NZ // 2 + (1 - 2 * lax.rem(ring, 2)) * ((ring + 1) // 2)
        return dz, i + i // (NKV - NY)

    def kv_peer(i):
        dz, dy = away(i)
        return lax.rem(z + dz, NZ) * NY + lax.rem(y + dy, NY)

    def tp_peer(i):
        return lax.rem(tp + 1 + i, NTP)

    barrier = pltpu.get_barrier_semaphore()

    def greet_kv(i, c):
        pl.semaphore_signal(barrier, 1, device_id=(kv_peer(i), tp), device_id_type=MESH)
        return c

    def greet_tp(i, c):
        pl.semaphore_signal(barrier, 1, device_id=(kv, tp_peer(i)), device_id_type=MESH)
        return c

    lax.fori_loop(0, NKV - 1, greet_kv, 0)
    lax.fori_loop(0, NTP - 1, greet_tp, 0)

    pair_cols = pl.ds(pl.multiple_of(kv // 2 * 128, 128), 128)
    loads = {
        "stream": (stream_hbm, stream_ref), "gain_in": (gain_in_hbm, gain_in_ref),
        "wf": (wf_hbm.at[:, pair_cols], wf), "wq": (wq_hbm, wq), "wk": (wk_hbm, wk),
        "wv": (wv_hbm, wv), "lengths": (lengths_hbm, lengths_ref),
        "decay": (decay_hbm, decay_ref), "keys": (keys_hbm, keys), "values": (values_hbm, values),
        "gain_att": (gain_att_hbm, gain_att_ref), "wo": (wo_hbm, wo),
        "gain_mlp": (gain_mlp_hbm, gain_mlp_ref), "wu": (wu_hbm, wu), "wd": (wd_hbm, wd),
    }
    loads = {
        name: pltpu.make_async_copy(a, b, load_sem.at[k])
        for k, (name, (a, b)) in enumerate(loads.items())
    }
    for load in loads.values():
        load.start()

    def loaded(*names):
        for name in names:
            loads[name].wait()

    lane = lax.broadcasted_iota(jnp.int32, (SEQS, 128), 1)
    low_half = lane < 64

    def to_kv(name, source, target):
        def step(i, c):
            peer = kv_peer(i)
            pltpu.make_async_remote_copy(
                src_ref=source(peer), dst_ref=target, send_sem=send_sem.at[name],
                recv_sem=recv_sem.at[name], device_id=(peer, tp), device_id_type=MESH,
            ).start()
            return c

        lax.fori_loop(0, NKV - 1, step, 0)

    def to_tp(name, source, target):
        def step(i, c):
            pltpu.make_async_remote_copy(
                src_ref=source, dst_ref=target, send_sem=send_sem.at[name],
                recv_sem=recv_sem.at[name], device_id=(kv, tp_peer(i)), device_id_type=MESH,
            ).start()
            return c

        lax.fori_loop(0, NTP - 1, step, 0)

    def arrived(name, buffer):
        n = buffer.shape[0] - 1
        whole = buffer.at[pl.ds(0, n)]
        pltpu.make_async_copy(whole, whole, recv_sem.at[name]).wait()

    def sent(name, buffer):
        n = buffer.shape[0] - 1
        whole = buffer.at[pl.ds(0, n)]
        pltpu.make_async_copy(whole, whole, send_sem.at[name]).wait()

    loaded("stream", "gain_in", "wf", "wq", "wk", "wv")
    stream = stream_ref[...].astype(f32)
    scaled = (stream * gain_in_ref[...].astype(f32)).astype(bf16)
    squares = jnp.sum(stream * stream, axis=1, keepdims=True)
    mine = low_half == (lax.rem(kv, 2) == 0)
    scaled_f = scaled.astype(f32)
    both = jnp.where(mine, jnp.concatenate([scaled_f, scaled_f], axis=1), 0.0).astype(bf16)
    part_f = lax.dot_general(both, wf[...], NT, preferred_element_type=f32)
    lane_f = lax.broadcasted_iota(jnp.int32, part_f.shape, 1)
    for r, w in enumerate((wq, wk, wv)):
        part = jnp.dot(scaled, w[...], preferred_element_type=f32)
        for h in range(HEADS):
            send1[h * SEQS : (h + 1) * SEQS, r, :] = part[:, h * HD : (h + 1) * HD]
    for h in range(HEADS):
        gate = jnp.sum(jnp.where(lane_f == tp * HEADS + h, part_f, 0.0), axis=1, keepdims=True)
        send1[h * SEQS : (h + 1) * SEQS, 3, :] = jnp.where(low_half, gate, squares)
    recv1[kv] = send1[kv]
    loaded("lengths", "decay")
    for s in range(SEQS):
        len_buf[s : s + 1, :] = jnp.full((1, 128), lengths_ref[s], jnp.int32)
    live = kv * POS + lane < len_buf[...]
    for h in range(HEADS):
        bias = jnp.where(live, decay_ref[:, h, :], MASKED)
        bias_buf[h * SEQS // NY : (h + 1) * SEQS // NY] = bias.reshape(SEQS // NY, NY, 128)
    loaded("keys", "values")
    pl.semaphore_wait(barrier, NKV - 1 + NTP - 1)
    to_kv(QKV, lambda peer: send1.at[peer], recv1.at[kv])
    arrived(QKV, recv1)
    total = jnp.sum(recv1[...], axis=0)
    extra = total[3:4, :]
    lane_1 = lax.broadcasted_iota(jnp.int32, (1, 128), 1)
    gate_sum = jnp.sum(jnp.where(lane_1 == 0, extra, 0.0), axis=1, keepdims=True)
    square_sum = jnp.sum(jnp.where(lane_1 == 127, extra, 0.0), axis=1, keepdims=True)
    scale_in = lax.rsqrt(square_sum / D + NORM_EPS)
    query = (total[0:1, :] * scale_in).astype(bf16).astype(f32)
    send_q[...] = query
    recv_q[kv] = query

    def send_query(i, c):
        dz, _ = away(i)
        pltpu.make_async_remote_copy(
            src_ref=send_q, dst_ref=recv_q.at[kv], send_sem=query_send_sem,
            recv_sem=query_sem.at[dz], device_id=(kv_peer(i), tp), device_id_type=MESH,
        ).start()
        return c

    lax.fori_loop(0, NKV - 1, send_query, 0)
    key_new = (total[1:2, :] * scale_in).astype(bf16).astype(f32)
    value_new = (total[2:3, :] * scale_in).astype(bf16).astype(f32)
    gate_in = gate_sum * scale_in
    forget = jnp.minimum(gate_in, 0.0) - jnp.log1p(jnp.exp(-jnp.abs(gate_in)))
    score_scale = 1.0 / math.sqrt(HD)
    own = jnp.sum(query * key_new, axis=1, keepdims=True) * score_scale

    def group(steps):
        zs = [lax.rem(z + NZ - dz, NZ) for dz in steps]
        pairs = []
        for dz, zs_ in zip(steps, zs):
            part = recv_q.at[pl.ds(0, NY if dz else NY - 1)]
            pltpu.make_async_copy(part, part, query_sem.at[dz]).wait()
            pairs += [(zs_ * NY + j, j, dz) for j in range(NY)]
        scores = []
        for p, _, _ in pairs:
            scores.append(
                lax.dot_general(
                    recv_q[p].astype(bf16), keys[lax.rem(p, SEQS), p // SEQS], NT,
                    preferred_element_type=f32,
                )
            )
        bias = jnp.concatenate([bias_buf[zs_] for zs_ in zs], axis=0)
        alive = bias > 0.5 * MASKED
        logits = jnp.concatenate(scores, axis=0) * score_scale + bias
        logits = jnp.where(alive, logits, MASKED)
        peak = jnp.max(logits, axis=1, keepdims=True)
        probs = jnp.where(alive, jnp.exp(logits - peak), 0.0)
        block_total = jnp.sum(probs, axis=1, keepdims=True)
        stats = jnp.where(low_half[: len(pairs)], peak, block_total)
        for k, (p, _, _) in enumerate(pairs):
            send2[p, 0:1, :] = jnp.dot(
                probs[k : k + 1].astype(bf16), values[lax.rem(p, SEQS), p // SEQS],
                preferred_element_type=f32,
            )
            send2[p, 1:2, :] = stats[k : k + 1]
        for p, j, dz in pairs:
            copy = pltpu.make_async_remote_copy(
                src_ref=send2.at[p], dst_ref=recv2.at[kv], send_sem=send_sem.at[PART],
                recv_sem=recv_sem.at[PART], device_id=(p, tp), device_id_type=MESH,
            )
            if dz:
                copy.start()
            else:
                pl.when(j != y)(copy.start)

    group([2, 14, 1, 15, 0])
    recv2[kv] = send2[kv]
    group([4, 12, 3, 13])
    group([6, 10, 5, 11])
    group([8, 7, 9])
    arrived(PART, recv2)
    block_out, stats = recv2[:, 0, :], recv2[:, 1, :]
    low = lax.broadcasted_iota(jnp.int32, (NKV, 128), 1) < 64
    peaks = jnp.max(jnp.where(low, stats, 2 * MASKED), axis=1, keepdims=True) + forget
    totals = jnp.max(jnp.where(low, 0.0, stats), axis=1, keepdims=True)
    top = jnp.maximum(own, jnp.max(peaks, axis=0, keepdims=True))
    weight = jnp.exp(peaks - top)
    own_weight = jnp.exp(own - top)
    numerator = jnp.sum(weight * block_out, axis=0, keepdims=True) + own_weight * value_new
    denominator = jnp.sum(weight * totals, axis=0, keepdims=True) + own_weight
    attended = numerator / denominator
    send_a[...] = attended
    recv_a[kv] = attended
    to_kv(ATT, lambda peer: send_a, recv_a.at[kv])
    loaded("wo", "gain_att", "gain_mlp", "wu", "wd")
    arrived(ATT, recv_a)

    part_out, att_squares = None, None
    for h in range(HEADS):
        att = recv_a[h * SEQS : (h + 1) * SEQS, 0, :]
        att_in = (att * gain_att_ref[h : h + 1, :].astype(f32)).astype(bf16)
        term = lax.dot_general(
            att_in, wo[:, h * HD : (h + 1) * HD], NT, preferred_element_type=f32
        )
        square = jnp.sum(att * att, axis=1, keepdims=True)
        part_out = term if h == 0 else part_out + term
        att_squares = square if h == 0 else att_squares + square
    row = lax.broadcasted_iota(jnp.int32, (SEQS, 128), 0)

    def as_row(column):
        return jnp.sum(jnp.where(row == lane, column, 0.0), axis=0, keepdims=True)

    def as_column(line):
        return jnp.sum(jnp.where(row == lane, line, 0.0), axis=1, keepdims=True)

    half = SEQS // 2
    send_o[...] = jnp.concatenate([part_out[:half], part_out[half:]], axis=1)
    send_os[...] = as_row(att_squares)
    recv_o[tp] = send_o[...]
    recv_os[tp] = send_os[...]
    to_tp(OUT, send_o, recv_o.at[tp])
    to_tp(OUT_SQ, send_os, recv_os.at[tp])
    arrived(OUT, recv_o)
    arrived(OUT_SQ, recv_os)
    out_total = jnp.sum(recv_o[...], axis=0)
    out_total = jnp.concatenate([out_total[:, :COLS], out_total[:, COLS:]], axis=0)
    scale_att = lax.rsqrt(as_column(jnp.sum(recv_os[...], axis=0)) / HW + NORM_EPS)
    residual = (stream + scale_att * out_total).astype(bf16).astype(f32)

    mixer_in = (residual * gain_mlp_ref[...].astype(f32)).astype(bf16)
    for u in range(BLOCKS):
        part = jnp.dot(mixer_in, wu[:, u * 128 : (u + 1) * 128], preferred_element_type=f32)
        send_u[u * 4 : (u + 1) * 4] = part.astype(bf16).reshape(4, 8, 128)
    recv_u[kv] = send_u[kv]
    to_kv(UP, lambda peer: send_u.at[peer], recv_u.at[kv])
    adder = lax.rem(kv, NTP) == tp
    send_s[...] = as_row(jnp.sum(residual * residual, axis=1, keepdims=True))

    def send_squares(j, c):
        peer = j * NTP + tp

        @pl.when(peer != kv)
        def _():
            pltpu.make_async_remote_copy(
                src_ref=send_s, dst_ref=recv_s.at[kv], send_sem=send_sem.at[SQUARES],
                recv_sem=recv_sem.at[SQUARES], device_id=(peer, tp), device_id_type=MESH,
            ).start()

        return c

    lax.fori_loop(0, NKV // NTP, send_squares, 0)
    arrived(UP, recv_u)
    active = jnp.maximum(jnp.sum(recv_u[...].astype(f32), axis=0), 0.0)
    hidden = (active * active).astype(bf16)
    send_h[...] = hidden
    recv_h[kv] = hidden
    to_kv(HIDDEN, lambda peer: send_h, recv_h.at[kv])

    @pl.when(adder)
    def _():
        arrived(SQUARES, recv_s)
        recv_s[kv] = send_s[...]
        recv_t[...] = jnp.sum(recv_s[...], axis=0)
        to_tp(SCALE, recv_t, recv_t)

    arrived(HIDDEN, recv_h)

    part_down = None
    for u in range(BLOCKS):
        term = lax.dot_general(
            recv_h[u * 4 : (u + 1) * 4].reshape(SEQS, 128), wd[:, u * 128 : (u + 1) * 128], NT,
            preferred_element_type=f32,
        )
        part_down = term if u == 0 else part_down + term
    send_d[...] = jnp.concatenate([part_down[:half], part_down[half:]], axis=1)
    recv_d[tp] = send_d[...]
    to_tp(DOWN, send_d, recv_d.at[tp])
    @pl.when(jnp.logical_not(adder))
    def _():
        pltpu.make_async_copy(recv_t, recv_t, recv_sem.at[SCALE]).wait()

    scale_mixer = lax.rsqrt(as_column(recv_t[...]) / D + NORM_EPS)
    arrived(DOWN, recv_d)
    down = jnp.sum(recv_d[...], axis=0)
    down = jnp.concatenate([down[:, :COLS], down[:, COLS:]], axis=0)
    out_ref[...] = (residual + scale_mixer * scale_mixer * down).astype(bf16)

    for name, buffer in (
        (QKV, recv1), (PART, recv2), (ATT, recv_a), (OUT, recv_o), (OUT_SQ, recv_os), (UP, recv_u),
        (HIDDEN, recv_h), (DOWN, recv_d),
    ):
        sent(name, buffer)
    queries = recv_q.at[pl.ds(0, NKV - 1)]
    pltpu.make_async_copy(queries, queries, query_send_sem).wait()
    rows_out = recv_s.at[pl.ds(0, NKV // NTP - 1)]
    pltpu.make_async_copy(rows_out, rows_out, send_sem.at[SQUARES]).wait()

    @pl.when(jnp.logical_not(adder))
    def _():
        pltpu.make_async_copy(send_s, send_s, send_sem.at[SQUARES]).wait()

    @pl.when(adder)
    def _():
        rows_out = recv_s.at[pl.ds(0, NTP - 1)]
        pltpu.make_async_copy(rows_out, rows_out, send_sem.at[SCALE]).wait()


def per_device(
    stream, gain_in, w_query, w_key, w_value, w_forget, keys_cache, values_cache, decay_cache,
    lengths, gain_att, w_out, gain_mlp, w_up, w_down,
):
    hbm = pl.BlockSpec(memory_space=pl.ANY)
    V = pltpu.VMEM
    scratch = [
        V((SEQS, COLS), bf16), V((1, COLS), bf16),
        V((COLS, HEADS * HD), bf16), V((COLS, HEADS * HD), bf16), V((COLS, HEADS * HD), bf16),
        V((16, 128), bf16),
        V((SEQS, HEADS, POS, HD), bf16), V((SEQS, HEADS, POS, HD), bf16),
        V((SEQS, HEADS, POS), f32), pltpu.SMEM((SEQS,), jnp.int32), V((HEADS, HD), bf16),
        V((COLS, HEADS * HD), bf16), V((1, COLS), bf16), V((COLS, UNITS), bf16),
        V((COLS, UNITS), bf16),
        V((SEQS, 128), jnp.int32), V((NZ, NY, 128), f32),
        V((NKV, 4, 128), f32), V((NKV, 4, 128), f32),
        V((1, 128), f32), V((NKV, 1, 128), f32),
        V((NKV, 2, 128), f32), V((NKV, 2, 128), f32),
        V((1, 128), f32), V((NKV, 1, 128), f32),
        V((SEQS // 2, 128), f32), V((NTP, SEQS // 2, 128), f32),
        V((1, 128), f32), V((NTP, 1, 128), f32),
        V((NKV, 8, 128), bf16), V((NKV, 8, 128), bf16),
        V((1, 128), f32), V((NKV, 1, 128), f32), V((1, 128), f32),
        V((8, 128), bf16), V((NKV, 8, 128), bf16),
        V((SEQS // 2, 128), f32), V((NTP, SEQS // 2, 128), f32),
        pltpu.SemaphoreType.DMA((15,)),
        pltpu.SemaphoreType.DMA((EXCHANGES,)), pltpu.SemaphoreType.DMA((EXCHANGES,)),
        pltpu.SemaphoreType.DMA, pltpu.SemaphoreType.DMA((NZ,)),
    ]
    return pl.pallas_call(
        kernel,
        out_shape=pltpu.VMEM((SEQS, COLS), bf16),
        in_specs=[hbm] * 15,
        out_specs=pl.BlockSpec(memory_space=pltpu.VMEM),
        scratch_shapes=scratch,
        compiler_params=pltpu.CompilerParams(collective_id=0, has_side_effects=True),
    )(
        stream, gain_in.reshape(1, COLS), w_query, w_key, w_value, w_forget.T, keys_cache,
        values_cache, decay_cache, lengths, gain_att.reshape(HEADS, HD), w_out.T,
        gain_mlp.reshape(1, COLS), w_up, w_down.T,
    )


def solution(mesh):
    return jax.shard_map(
        per_device,
        mesh=mesh,
        in_specs=(
            P(None, "kv"), P("kv"), P("kv", "tp"), P("kv", "tp"), P("kv", "tp"), P(),
            P(None, "tp", "kv", None), P(None, "tp", "kv", None), P(None, "tp", "kv"), P(),
            P("tp"), P("tp", "kv"), P("kv"), P("kv", "tp"), P("tp", "kv"),
        ),
        out_specs=P(None, "kv"),
        check_vma=False,
    )
```

time: 94.9 us -> 82.6 us (0.87)
  local copies, waits for them, and re-layouts: 6.99 us -> 0.6 us
  Pallas kernels: 87.6 us -> 81.9 us
    unnamed x4 -> x1, local copies, waits for them, and re-layouts: 6.99 us -> 0.6 us
    pallas_call x1, Pallas kernels: 87.6 us -> 81.9 us  [per_device(): pl.pallas_call(kernel, out_shape=pltpu.VMEM((SEQS, COLS), bf16), in_specs...]
where the time goes in v2:
time: 82.6 us; the launch traced here: 82.5 us
  Pallas kernels  81.9 us (99%)
    pallas_call x1, Pallas kernels, per_device(): pl.pallas_call(kernel, out_shape=pltpu.VMEM((SEQS, COLS), bf16), in_specs...  81.9 us

profile of v2, /device:TPU:1, one launch (start us, length us, event | category | flops | bytes accessed | tf_op | source)
XLA Modules:
  0.0 82.5 jit_solution(3629674351198410762)
XLA Ops:
  0.0 81.9 %shard_map.145 = bf16[32,64]{1,0:T(8,128)(2,1)S(1)} custom-call(bf16[32,64]{1,0:T(8,128)(2,1)} %stream_hbm.1, bf16[1,64]{1,0:T(2,128)(2,1)} %bitcast.9, bf16[64,256]{1,0:T(8,128)(2,1)} %wq_hbm.1, bf16[64,256]{1,0:T(8,128)(2,1)} %wk_hbm.1, bf16[64,256]{1,0:T(8,128)(2,1)} %wv_hbm.1, bf16[16,4096]{1,0:T(8,128)(2,1)} %bitcast.7, ...), custom_call_target="tpu_custom_call" | custom-call | tf_op jit(solution)/shard_map/pallas_call | solution.py:374
  81.9 0.6 copy.17

commit v3 on v2

v3 whole, which is shorter than its diff:
```python
import math

import jax
import jax.numpy as jnp
from jax import lax
from jax.experimental import pallas as pl
from jax.experimental.pallas import tpu as pltpu
from jax.sharding import PartitionSpec as P

f32, bf16 = jnp.float32, jnp.bfloat16
MESH = pl.DeviceIdType.MESH
NORM_EPS = 1e-06
MASKED = -1e30
NT = (((1,), (1,)), ((), ()))

NZ, NY, NTP = 16, 4, 8
NKV = NZ * NY
GROUP = 16
FARS = NKV // GROUP
SEQS, HEADS, HD, POS = 32, 2, 128, 128
COLS, UNITS = 64, 2048
D, HW = NKV * COLS, NTP * HEADS * HD
BLOCKS = UNITS // 128

(
    QUERY_IN, REST_IN, SQ_IN, FAR_SQ_IN, QUERY, FAR_REST, PART, ATT, OUT, OUT_SQ,
    UP, SQ_MIX, FAR_UP, FAR_SQ_MIX, HIDDEN, DOWN,
) = range(16)
EXCHANGES = 16


def kernel(
    stream_hbm, gain_in_hbm, wq_hbm, wk_hbm, wv_hbm, wf_hbm, keys_hbm, values_hbm, decay_hbm,
    lengths_hbm, gain_att_hbm, wo_hbm, gain_mlp_hbm, wu_hbm, wd_hbm,
    out_ref,
    stream_ref, gain_in_ref, wq, wk, wv, wf, keys, values, decay_ref, lengths_ref, gain_att_ref,
    wo, gain_mlp_ref, wu, wd,
    len_buf, bias_buf, query_buf,
    send_qi, recv_qi, send_ri, recv_ri, send_si, recv_si, send_fsi, recv_fsi, send_q, recv_q, send_fr, recv_fr, rest_buf,
    send2, recv2, send_a, recv_a, send_o, recv_o, send_os, recv_os,
    send_u, recv_u, send_sm, recv_sm, send_fu, recv_fu, send_fsm, recv_fsm, send_h, recv_h,
    send_d, recv_d,
    load_sem, send_sem, recv_sem,
):
    kv, tp = lax.axis_index("kv"), lax.axis_index("tp")
    z, y = kv // NY, lax.rem(kv, NY)
    far, near = kv // GROUP, lax.rem(kv, GROUP)

    def kv_peer(i):
        ring = i // NY
        dz = NZ // 2 + (1 - 2 * lax.rem(ring, 2)) * ((ring + 1) // 2)
        dy = i + i // (NKV - NY)
        return lax.rem(z + dz, NZ) * NY + lax.rem(y + dy, NY)

    def tp_peer(i):
        return lax.rem(tp + 1 + i, NTP)

    barrier = pltpu.get_barrier_semaphore()

    def greet(kv_to, tp_to):
        pl.semaphore_signal(barrier, 1, device_id=(kv_to, tp_to), device_id_type=MESH)

    def greet_line(i, c):
        greet(lax.rem(z // 4 * 4 + 4 + lax.rem(i + 4, NZ - 4), NZ) * NY + y, tp)
        return c

    def greet_group(i, c):
        greet(far * GROUP + lax.rem(near + 1 + i, GROUP), tp)
        return c

    def greet_tp(i, c):
        greet(kv, tp_peer(i))
        return c

    lax.fori_loop(0, NZ - 4, greet_line, 0)
    lax.fori_loop(0, GROUP - 1, greet_group, 0)
    lax.fori_loop(0, NTP - 1, greet_tp, 0)

    pair_cols = pl.ds(pl.multiple_of(kv // 2 * 128, 128), 128)
    loads = {
        "stream": (stream_hbm, stream_ref), "gain_in": (gain_in_hbm, gain_in_ref),
        "wf": (wf_hbm.at[:, pair_cols], wf), "wq": (wq_hbm, wq), "wk": (wk_hbm, wk),
        "wv": (wv_hbm, wv), "lengths": (lengths_hbm, lengths_ref),
        "decay": (decay_hbm, decay_ref), "keys": (keys_hbm, keys), "values": (values_hbm, values),
        "gain_att": (gain_att_hbm, gain_att_ref), "wo": (wo_hbm, wo),
        "gain_mlp": (gain_mlp_hbm, gain_mlp_ref), "wu": (wu_hbm, wu), "wd": (wd_hbm, wd),
    }
    loads = {
        name: pltpu.make_async_copy(a, b, load_sem.at[k])
        for k, (name, (a, b)) in enumerate(loads.items())
    }
    for load in loads.values():
        load.start()

    def loaded(*names):
        for name in names:
            loads[name].wait()

    lane = lax.broadcasted_iota(jnp.int32, (SEQS, 128), 1)
    low_half = lane < 64

    def put(name, source, target, peer):
        pltpu.make_async_remote_copy(
            src_ref=source, dst_ref=target, send_sem=send_sem.at[name],
            recv_sem=recv_sem.at[name], device_id=(peer, tp), device_id_type=MESH,
        ).start()

    def to_kv(name, source, target):
        def step(i, c):
            put(name, source, target, kv_peer(i))
            return c

        lax.fori_loop(0, NKV - 1, step, 0)

    def to_group(name, source, target):
        def step(i, c):
            to = lax.rem(near + 1 + i, GROUP)
            put(name, source(to), target, far * GROUP + to)
            return c

        lax.fori_loop(0, GROUP - 1, step, 0)

    def to_far(name, source, target):
        for i in (2, 1, 3):
            to = lax.rem(far + i, FARS)
            put(name, source(to), target, to * GROUP + near)

    def to_tp(name, source, target):
        def step(i, c):
            pltpu.make_async_remote_copy(
                src_ref=source, dst_ref=target, send_sem=send_sem.at[name],
                recv_sem=recv_sem.at[name], device_id=(kv, tp_peer(i)), device_id_type=MESH,
            ).start()
            return c

        lax.fori_loop(0, NTP - 1, step, 0)

    def arrived(name, buffer):
        n = buffer.shape[0] - 1
        whole = buffer.at[pl.ds(0, n)]
        pltpu.make_async_copy(whole, whole, recv_sem.at[name]).wait()

    def sent(name, buffer):
        n = buffer.shape[0] - 1
        whole = buffer.at[pl.ds(0, n)]
        pltpu.make_async_copy(whole, whole, send_sem.at[name]).wait()

    row = lax.broadcasted_iota(jnp.int32, (SEQS, 128), 0)

    def as_row(column):
        return jnp.sum(jnp.where(row == lane, column, 0.0), axis=0, keepdims=True)

    def as_column(line):
        return jnp.sum(jnp.where(row == lane, line, 0.0), axis=1, keepdims=True)

    loaded("stream", "gain_in", "wf", "wq", "wk", "wv")
    stream = stream_ref[...].astype(f32)
    scaled = (stream * gain_in_ref[...].astype(f32)).astype(bf16)
    squares = jnp.sum(stream * stream, axis=1, keepdims=True)
    mine = low_half == (lax.rem(kv, 2) == 0)
    scaled_f = scaled.astype(f32)
    both = jnp.where(mine, jnp.concatenate([scaled_f, scaled_f], axis=1), 0.0).astype(bf16)
    part_f = lax.dot_general(both, wf[...], NT, preferred_element_type=f32)
    lane_f = lax.broadcasted_iota(jnp.int32, part_f.shape, 1)
    for r, w in enumerate((wq, wk, wv)):
        part = jnp.dot(scaled, w[...], preferred_element_type=f32)
        for h in range(HEADS):
            block = part[:, h * HD : (h + 1) * HD].reshape(SEQS // 4, 4, 128)
            if r == 0:
                send_qi[h * SEQS // 4 : (h + 1) * SEQS // 4] = block
            else:
                send_ri[h * SEQS // 4 : (h + 1) * SEQS // 4, r - 1] = block
    for h in range(HEADS):
        gate = jnp.sum(jnp.where(lane_f == tp * HEADS + h, part_f, 0.0), axis=1, keepdims=True)
        block = jnp.broadcast_to(gate, (SEQS, 128)).reshape(SEQS // 4, 4, 128)
        send_ri[h * SEQS // 4 : (h + 1) * SEQS // 4, 2] = block
    recv_qi[near] = send_qi[near]
    recv_ri[near] = send_ri[near]
    send_si[...] = as_row(squares)
    recv_si[near] = send_si[...]
    pl.semaphore_wait(barrier, NZ - 4 + GROUP - 1 + NTP - 1)
    to_group(SQ_IN, lambda to: send_si, recv_si.at[near])
    to_group(QUERY_IN, lambda to: send_qi.at[to], recv_qi.at[near])
    to_group(REST_IN, lambda to: send_ri.at[to], recv_ri.at[near])
    loaded("lengths", "decay")
    for s in range(SEQS):
        len_buf[s : s + 1, :] = jnp.full((1, 128), lengths_ref[s], jnp.int32)
    live = kv * POS + lane < len_buf[...]
    for h in range(HEADS):
        bias = jnp.where(live, decay_ref[:, h, :], MASKED)
        bias_buf[h * SEQS // NY : (h + 1) * SEQS // NY] = bias.reshape(SEQS // NY, NY, 128)
    loaded("keys", "values")
    arrived(SQ_IN, recv_si)
    send_fsi[...] = jnp.sum(recv_si[...], axis=0)
    recv_fsi[far] = send_fsi[...]
    to_far(FAR_SQ_IN, lambda to: send_fsi, recv_fsi.at[far])
    arrived(QUERY_IN, recv_qi)
    send_q[...] = jnp.sum(recv_qi[...], axis=0)
    recv_q[kv] = send_q[...]
    to_kv(QUERY, send_q, recv_q.at[kv])
    arrived(REST_IN, recv_ri)
    send_fr[...] = jnp.sum(recv_ri[...], axis=0)
    recv_fr[far] = send_fr[...]
    to_far(FAR_REST, lambda to: send_fr, recv_fr.at[far])
    arrived(FAR_SQ_IN, recv_fsi)
    scale_in = lax.rsqrt(as_column(jnp.sum(recv_fsi[...], axis=0)) / D + NORM_EPS)
    scale_rows = jnp.broadcast_to(scale_in, (SEQS, 128)).reshape(SEQS // 4, 4, 128)
    arrived(QUERY, recv_q)
    for h in range(HEADS):
        rows = 0.0
        for f in range(FARS):
            at = f * GROUP + h * SEQS // 4
            rows = rows + recv_q[at : at + SEQS // 4]
        rows = (rows * scale_rows).astype(bf16).astype(f32)
        query_buf[h * SEQS // 4 : (h + 1) * SEQS // 4] = rows
    score_scale = 1.0 / math.sqrt(HD)

    def part(steps):
        pairs = []
        for dz in steps:
            ring = lax.rem(z + dz, NZ)
            for j in range(NY):
                owner = ring * NY + j
                to, of = lax.rem(owner, GROUP), owner // GROUP
                at = (lax.rem(to, SEQS // 4) * 4 + of, to // (SEQS // 4))
                pairs.append((owner, to, of, at, dz, j))
        scores, biases = [], []
        for _, to, of, at, _, _ in pairs:
            q = query_buf[to, pl.ds(of, 1), :].astype(bf16)
            scores.append(lax.dot_general(q, keys[at], NT, preferred_element_type=f32))
            biases.append(bias_buf[to, pl.ds(of, 1), :])
        bias = jnp.concatenate(biases, axis=0)
        alive = bias > 0.5 * MASKED
        logits = jnp.concatenate(scores, axis=0) * score_scale + bias
        logits = jnp.where(alive, logits, MASKED)
        peak = jnp.max(logits, axis=1, keepdims=True)
        probs = jnp.where(alive, jnp.exp(logits - peak), 0.0)
        block_total = jnp.sum(probs, axis=1, keepdims=True)
        stats = jnp.where(low_half[: len(pairs)], peak, block_total)
        for k, (owner, _, _, at, _, _) in enumerate(pairs):
            send2[owner, 0:1, :] = jnp.dot(
                probs[k : k + 1].astype(bf16), values[at], preferred_element_type=f32
            )
            send2[owner, 1:2, :] = stats[k : k + 1]
        for owner, _, _, _, dz, j in pairs:
            send = lambda owner=owner: put(PART, send2.at[owner], recv2.at[kv], owner)
            if dz:
                send()
            else:
                pl.when(j != y)(send)

    part([8, 7, 9])
    part([6, 10, 5, 11])
    part([4, 12, 3, 13])
    part([2, 14, 1, 15, 0])
    recv2[kv] = send2[kv]
    arrived(FAR_REST, recv_fr)
    rest_buf[...] = jnp.sum(recv_fr[...], axis=0)
    lane_1 = lax.broadcasted_iota(jnp.int32, (1, 128), 1)
    my_seq = lax.rem(near, SEQS // 4) * 4 + far
    square_line = jnp.sum(recv_fsi[...], axis=0)
    square_sum = jnp.sum(jnp.where(lane_1 == my_seq, square_line, 0.0), axis=1, keepdims=True)
    my_scale = lax.rsqrt(square_sum / D + NORM_EPS)
    query = query_buf[near, pl.ds(far, 1), :]
    key_new = (rest_buf[0, pl.ds(far, 1), :] * my_scale).astype(bf16).astype(f32)
    value_new = (rest_buf[1, pl.ds(far, 1), :] * my_scale).astype(bf16).astype(f32)
    gate_in = rest_buf[2, pl.ds(far, 1), :][:, 0:1] * my_scale
    forget = jnp.minimum(gate_in, 0.0) - jnp.log1p(jnp.exp(-jnp.abs(gate_in)))
    own = jnp.sum(query * key_new, axis=1, keepdims=True) * score_scale
    arrived(PART, recv2)
    block_out, stats = recv2[:, 0, :], recv2[:, 1, :]
    low = lax.broadcasted_iota(jnp.int32, (NKV, 128), 1) < 64
    peaks = jnp.max(jnp.where(low, stats, 2 * MASKED), axis=1, keepdims=True)
    totals = jnp.max(jnp.where(low, 0.0, stats), axis=1, keepdims=True)
    own = own - forget
    top = jnp.maximum(own, jnp.max(peaks, axis=0, keepdims=True))
    weight = jnp.exp(peaks - top)
    own_weight = jnp.exp(own - top)
    numerator = jnp.sum(weight * block_out, axis=0, keepdims=True) + own_weight * value_new
    denominator = jnp.sum(weight * totals, axis=0, keepdims=True) + own_weight
    attended = numerator / denominator
    send_a[...] = attended
    my_pair = near * 4 + far
    recv_a[my_pair] = attended
    to_kv(ATT, send_a, recv_a.at[my_pair])
    loaded("wo", "gain_att", "gain_mlp", "wu", "wd")
    arrived(ATT, recv_a)

    part_out, att_squares = None, None
    for h in range(HEADS):
        att = recv_a[h * SEQS : (h + 1) * SEQS, 0, :]
        att_in = (att * gain_att_ref[h : h + 1, :].astype(f32)).astype(bf16)
        term = lax.dot_general(
            att_in, wo[:, h * HD : (h + 1) * HD], NT, preferred_element_type=f32
        )
        square = jnp.sum(att * att, axis=1, keepdims=True)
        part_out = term if h == 0 else part_out + term
        att_squares = square if h == 0 else att_squares + square
    half = SEQS // 2
    send_o[...] = jnp.concatenate([part_out[:half], part_out[half:]], axis=1)
    send_os[...] = as_row(att_squares)
    recv_o[tp] = send_o[...]
    recv_os[tp] = send_os[...]
    to_tp(OUT, send_o, recv_o.at[tp])
    to_tp(OUT_SQ, send_os, recv_os.at[tp])
    arrived(OUT, recv_o)
    arrived(OUT_SQ, recv_os)
    out_total = jnp.sum(recv_o[...], axis=0)
    out_total = jnp.concatenate([out_total[:, :COLS], out_total[:, COLS:]], axis=0)
    scale_att = lax.rsqrt(as_column(jnp.sum(recv_os[...], axis=0)) / HW + NORM_EPS)
    residual = (stream + scale_att * out_total).astype(bf16).astype(f32)

    mixer_in = (residual * gain_mlp_ref[...].astype(f32)).astype(bf16)
    send_sm[...] = as_row(jnp.sum(residual * residual, axis=1, keepdims=True))
    recv_sm[near] = send_sm[...]
    to_group(SQ_MIX, lambda to: send_sm, recv_sm.at[near])
    for u in range(BLOCKS):
        part = jnp.dot(mixer_in, wu[:, u * 128 : (u + 1) * 128], preferred_element_type=f32)
        send_u[u] = part.astype(bf16)
    recv_u[near] = send_u[near]
    to_group(UP, lambda to: send_u.at[to], recv_u.at[near])
    arrived(SQ_MIX, recv_sm)
    send_fsm[...] = jnp.sum(recv_sm[...], axis=0)
    recv_fsm[far] = send_fsm[...]
    to_far(FAR_SQ_MIX, lambda to: send_fsm, recv_fsm.at[far])
    arrived(UP, recv_u)
    group_sum = jnp.sum(recv_u[...].astype(f32), axis=0)
    send_fu[...] = group_sum.astype(bf16)
    recv_fu[far] = send_fu[...]
    to_far(FAR_UP, lambda to: send_fu, recv_fu.at[far])
    arrived(FAR_SQ_MIX, recv_fsm)
    scale_mixer = lax.rsqrt(as_column(jnp.sum(recv_fsm[...], axis=0)) / D + NORM_EPS)
    arrived(FAR_UP, recv_fu)
    active = jnp.maximum(jnp.sum(recv_fu[...].astype(f32), axis=0) * scale_mixer, 0.0)
    hidden = (active * active).astype(bf16)
    send_h[...] = hidden
    recv_h[near] = hidden
    to_group(HIDDEN, lambda to: send_h, recv_h.at[near])

    arrived(HIDDEN, recv_h)

    hidden_all = jnp.concatenate([recv_h[u] for u in range(BLOCKS)], axis=1)
    part_down = lax.dot_general(hidden_all, wd[...], NT, preferred_element_type=f32)
    send_d[...] = jnp.concatenate([part_down[:half], part_down[half:]], axis=1)
    recv_d[tp] = send_d[...]
    to_tp(DOWN, send_d, recv_d.at[tp])
    arrived(DOWN, recv_d)
    down = jnp.sum(recv_d[...], axis=0)
    down = jnp.concatenate([down[:, :COLS], down[:, COLS:]], axis=0)
    out_ref[...] = (residual + down).astype(bf16)

    for name, buffer in (
        (QUERY_IN, recv_qi), (REST_IN, recv_ri), (SQ_IN, recv_si), (FAR_SQ_IN, recv_fsi),
        (QUERY, recv_q), (FAR_REST, recv_fr),
        (PART, recv2), (ATT, recv_a), (OUT, recv_o), (OUT_SQ, recv_os), (UP, recv_u),
        (SQ_MIX, recv_sm), (FAR_UP, recv_fu), (FAR_SQ_MIX, recv_fsm), (HIDDEN, recv_h),
        (DOWN, recv_d),
    ):
        sent(name, buffer)


def per_device(
    stream, gain_in, w_query, w_key, w_value, w_forget, keys_cache, values_cache, decay_cache,
    lengths, gain_att, w_out, gain_mlp, w_up, w_down,
):
    hbm = pl.BlockSpec(memory_space=pl.ANY)
    V = pltpu.VMEM
    scratch = [
        V((SEQS, COLS), bf16), V((1, COLS), bf16),
        V((COLS, HEADS * HD), bf16), V((COLS, HEADS * HD), bf16), V((COLS, HEADS * HD), bf16),
        V((16, 128), bf16),
        V((SEQS, HEADS, POS, HD), bf16), V((SEQS, HEADS, POS, HD), bf16),
        V((SEQS, HEADS, POS), f32), pltpu.SMEM((SEQS,), jnp.int32), V((HEADS, HD), bf16),
        V((COLS, HEADS * HD), bf16), V((1, COLS), bf16), V((COLS, UNITS), bf16),
        V((COLS, UNITS), bf16),
        V((SEQS, 128), jnp.int32), V((NKV // 4, 4, 128), f32), V((NKV // 4, 4, 128), f32),
        V((GROUP, 4, 128), f32), V((GROUP, 4, 128), f32),
        V((GROUP, 3, 4, 128), f32), V((GROUP, 3, 4, 128), f32),
        V((1, 128), f32), V((GROUP, 1, 128), f32), V((1, 128), f32), V((FARS, 1, 128), f32),
        V((4, 128), f32), V((NKV, 4, 128), f32), V((3, 4, 128), f32), V((FARS, 3, 4, 128), f32),
        V((3, 4, 128), f32),
        V((NKV, 2, 128), f32), V((NKV, 2, 128), f32),
        V((1, 128), f32), V((NKV, 1, 128), f32),
        V((SEQS // 2, 128), f32), V((NTP, SEQS // 2, 128), f32),
        V((1, 128), f32), V((NTP, 1, 128), f32),
        V((BLOCKS, SEQS, 128), bf16), V((GROUP, SEQS, 128), bf16),
        V((1, 128), f32), V((GROUP, 1, 128), f32),
        V((SEQS, 128), bf16), V((FARS, SEQS, 128), bf16), V((1, 128), f32), V((FARS, 1, 128), f32),
        V((SEQS, 128), bf16), V((GROUP, SEQS, 128), bf16),
        V((SEQS // 2, 128), f32), V((NTP, SEQS // 2, 128), f32),
        pltpu.SemaphoreType.DMA((15,)),
        pltpu.SemaphoreType.DMA((EXCHANGES,)), pltpu.SemaphoreType.DMA((EXCHANGES,)),
    ]
    return pl.pallas_call(
        kernel,
        out_shape=pltpu.VMEM((SEQS, COLS), bf16),
        in_specs=[hbm] * 15,
        out_specs=pl.BlockSpec(memory_space=pltpu.VMEM),
        scratch_shapes=scratch,
        compiler_params=pltpu.CompilerParams(collective_id=0, has_side_effects=True),
    )(
        stream, gain_in.reshape(1, COLS), w_query, w_key, w_value, w_forget.T, keys_cache,
        values_cache, decay_cache, lengths, gain_att.reshape(HEADS, HD), w_out.T,
        gain_mlp.reshape(1, COLS), w_up, w_down.T,
    )


def solution(mesh):
    return jax.shard_map(
        per_device,
        mesh=mesh,
        in_specs=(
            P(None, "kv"), P("kv"), P("kv", "tp"), P("kv", "tp"), P("kv", "tp"), P(),
            P(None, "tp", "kv", None), P(None, "tp", "kv", None), P(None, "tp", "kv"), P(),
            P("tp"), P("tp", "kv"), P("kv"), P("kv", "tp"), P("tp", "kv"),
        ),
        out_specs=P(None, "kv"),
        check_vma=False,
    )
```

time: 82.6 us -> 76.4 us (0.925)
  Pallas kernels: 81.9 us -> 75.6 us
    pallas_call x1, Pallas kernels: 81.9 us -> 75.6 us  [per_device(): pl.pallas_call(kernel, out_shape=pltpu.VMEM((SEQS, COLS), bf16), in_specs...]
where the time goes in v3:
time: 76.4 us; the launch traced here: 76.2 us
  Pallas kernels  75.6 us (99%)
    pallas_call x1, Pallas kernels, per_device(): pl.pallas_call(kernel, out_shape=pltpu.VMEM((SEQS, COLS), bf16), in_specs...  75.6 us

profile of v3, /device:TPU:1, one launch (start us, length us, event | category | flops | bytes accessed | tf_op | source)
XLA Modules:
  0.0 76.2 jit_solution(1474106489174053353)
XLA Ops:
  0.0 75.6 %shard_map.145 = bf16[32,64]{1,0:T(8,128)(2,1)S(1)} custom-call(bf16[32,64]{1,0:T(8,128)(2,1)} %stream_hbm.1, bf16[1,64]{1,0:T(2,128)(2,1)} %bitcast.9, bf16[64,256]{1,0:T(8,128)(2,1)} %wq_hbm.1, bf16[64,256]{1,0:T(8,128)(2,1)} %wk_hbm.1, bf16[64,256]{1,0:T(8,128)(2,1)} %wv_hbm.1, bf16[16,4096]{1,0:T(8,128)(2,1)} %bitcast.7, ...), custom_call_target="tpu_custom_call" | custom-call | tf_op jit(solution)/shard_map/pallas_call | solution.py:394
  75.6 0.6 copy.17

commit v4 on v3

--- a/solution.py
+++ b/solution.py
@@ -27,6 +27,7 @@
     UP, SQ_MIX, FAR_UP, FAR_SQ_MIX, HIDDEN, DOWN,
 ) = range(16)
 EXCHANGES = 16
+HOME = (FAR_SQ_IN, FAR_REST, OUT, OUT_SQ, FAR_UP, FAR_SQ_MIX, DOWN)
 
 
 def kernel(
@@ -40,17 +41,17 @@
     send2, recv2, send_a, recv_a, send_o, recv_o, send_os, recv_os,
     send_u, recv_u, send_sm, recv_sm, send_fu, recv_fu, send_fsm, recv_fsm, send_h, recv_h,
     send_d, recv_d,
-    load_sem, send_sem, recv_sem,
+    load_sem, send_sem, recv_sem, seen_sem, opposite_sem,
 ):
     kv, tp = lax.axis_index("kv"), lax.axis_index("tp")
     z, y = kv // NY, lax.rem(kv, NY)
     far, near = kv // GROUP, lax.rem(kv, GROUP)
+    other = tp + 1 - 2 * lax.rem(tp, 2)
 
     def kv_peer(i):
         ring = i // NY
         dz = NZ // 2 + (1 - 2 * lax.rem(ring, 2)) * ((ring + 1) // 2)
-        dy = i + i // (NKV - NY)
-        return lax.rem(z + dz, NZ) * NY + lax.rem(y + dy, NY)
+        return lax.rem(z + dz, NZ) * NY + lax.rem(y + i, NY)
 
     def tp_peer(i):
         return lax.rem(tp + 1 + i, NTP)
@@ -60,20 +61,18 @@
     def greet(kv_to, tp_to):
         pl.semaphore_signal(barrier, 1, device_id=(kv_to, tp_to), device_id_type=MESH)
 
-    def greet_line(i, c):
-        greet(lax.rem(z // 4 * 4 + 4 + lax.rem(i + 4, NZ - 4), NZ) * NY + y, tp)
-        return c
-
     def greet_group(i, c):
-        greet(far * GROUP + lax.rem(near + 1 + i, GROUP), tp)
+        greet(far * GROUP + lax.rem(near + 1 + i, GROUP), other)
         return c
 
     def greet_tp(i, c):
         greet(kv, tp_peer(i))
         return c
 
-    lax.fori_loop(0, NZ - 4, greet_line, 0)
-    lax.fori_loop(0, GROUP - 1, greet_group, 0)
+    after, before = lax.rem(kv + GROUP, NKV), lax.rem(kv + NKV - GROUP, NKV)
+    greet(after, tp)
+    greet(before, tp)
+    lax.fori_loop(0, GROUP, greet_group, 0)
     lax.fori_loop(0, NTP - 1, greet_tp, 0)
 
     pair_cols = pl.ds(pl.multiple_of(kv // 2 * 128, 128), 128)
@@ -99,31 +98,31 @@
     lane = lax.broadcasted_iota(jnp.int32, (SEQS, 128), 1)
     low_half = lane < 64
 
-    def put(name, source, target, peer):
+    def put(name, source, target, peer, core):
         pltpu.make_async_remote_copy(
             src_ref=source, dst_ref=target, send_sem=send_sem.at[name],
-            recv_sem=recv_sem.at[name], device_id=(peer, tp), device_id_type=MESH,
+            recv_sem=recv_sem.at[name], device_id=(peer, core), device_id_type=MESH,
         ).start()
 
     def to_kv(name, source, target):
         def step(i, c):
-            put(name, source, target, kv_peer(i))
+            put(name, source, target, kv_peer(i), other)
             return c
 
-        lax.fori_loop(0, NKV - 1, step, 0)
+        lax.fori_loop(0, NKV, step, 0)
 
     def to_group(name, source, target):
         def step(i, c):
             to = lax.rem(near + 1 + i, GROUP)
-            put(name, source(to), target, far * GROUP + to)
+            put(name, source(to), target, far * GROUP + to, other)
             return c
 
-        lax.fori_loop(0, GROUP - 1, step, 0)
-
-    def to_far(name, source, target):
-        for i in (2, 1, 3):
+        lax.fori_loop(0, GROUP, step, 0)
+
+    def to_far(name, source, target, steps=(2, 1, 3)):
+        for i in steps:
             to = lax.rem(far + i, FARS)
-            put(name, source(to), target, to * GROUP + near)
+            put(name, source(to), target, to * GROUP + near, tp)
 
     def to_tp(name, source, target):
         def step(i, c):
@@ -136,12 +135,12 @@
         lax.fori_loop(0, NTP - 1, step, 0)
 
     def arrived(name, buffer):
-        n = buffer.shape[0] - 1
+        n = buffer.shape[0] - (name in HOME)
         whole = buffer.at[pl.ds(0, n)]
         pltpu.make_async_copy(whole, whole, recv_sem.at[name]).wait()
 
     def sent(name, buffer):
-        n = buffer.shape[0] - 1
+        n = buffer.shape[0] - (name in HOME)
         whole = buffer.at[pl.ds(0, n)]
         pltpu.make_async_copy(whole, whole, send_sem.at[name]).wait()
 
@@ -174,11 +173,10 @@
         gate = jnp.sum(jnp.where(lane_f == tp * HEADS + h, part_f, 0.0), axis=1, keepdims=True)
         block = jnp.broadcast_to(gate, (SEQS, 128)).reshape(SEQS // 4, 4, 128)
         send_ri[h * SEQS // 4 : (h + 1) * SEQS // 4, 2] = block
-    recv_qi[near] = send_qi[near]
-    recv_ri[near] = send_ri[near]
     send_si[...] = as_row(squares)
-    recv_si[near] = send_si[...]
-    pl.semaphore_wait(barrier, NZ - 4 + GROUP - 1 + NTP - 1)
+    pl.semaphore_wait(barrier, 2 + GROUP + NTP - 1)
+    for to in (after, before):
+        pl.semaphore_signal(seen_sem, 1, device_id=(to, tp), device_id_type=MESH)
     to_group(SQ_IN, lambda to: send_si, recv_si.at[near])
     to_group(QUERY_IN, lambda to: send_qi.at[to], recv_qi.at[near])
     to_group(REST_IN, lambda to: send_ri.at[to], recv_ri.at[near])
@@ -190,16 +188,30 @@
         bias = jnp.where(live, decay_ref[:, h, :], MASKED)
         bias_buf[h * SEQS // NY : (h + 1) * SEQS // NY] = bias.reshape(SEQS // NY, NY, 128)
     loaded("keys", "values")
+    pl.semaphore_wait(seen_sem, 2)
+    pl.semaphore_signal(opposite_sem, 1, device_id=(before, tp), device_id_type=MESH)
     arrived(SQ_IN, recv_si)
     send_fsi[...] = jnp.sum(recv_si[...], axis=0)
     recv_fsi[far] = send_fsi[...]
-    to_far(FAR_SQ_IN, lambda to: send_fsi, recv_fsi.at[far])
+    to_far(FAR_SQ_IN, lambda to: send_fsi, recv_fsi.at[far], (1, 3))
     arrived(QUERY_IN, recv_qi)
     send_q[...] = jnp.sum(recv_qi[...], axis=0)
-    recv_q[kv] = send_q[...]
+
+    def beside(i, c):
+        group = lax.rem(far + 1 + 2 * lax.rem(i, 2), FARS)
+        put(QUERY, send_q, recv_q.at[kv], group * GROUP + i // 2, other)
+        return c
+
+    def across(i, c):
+        put(QUERY, send_q, recv_q.at[kv], lax.rem(far + 2, FARS) * GROUP + i, other)
+        return c
+
+    pl.semaphore_wait(opposite_sem, 1)
+    to_far(FAR_SQ_IN, lambda to: send_fsi, recv_fsi.at[far], (2,))
     to_kv(QUERY, send_q, recv_q.at[kv])
     arrived(REST_IN, recv_ri)
-    send_fr[...] = jnp.sum(recv_ri[...], axis=0)
+    send_fr[:3] = jnp.sum(recv_ri[...], axis=0)
+    send_fr[3] = send_q[...]
     recv_fr[far] = send_fr[...]
     to_far(FAR_REST, lambda to: send_fr, recv_fr.at[far])
     arrived(FAR_SQ_IN, recv_fsi)
@@ -223,9 +235,9 @@
                 owner = ring * NY + j
                 to, of = lax.rem(owner, GROUP), owner // GROUP
                 at = (lax.rem(to, SEQS // 4) * 4 + of, to // (SEQS // 4))
-                pairs.append((owner, to, of, at, dz, j))
+                pairs.append((owner, to, of, at))
         scores, biases = [], []
-        for _, to, of, at, _, _ in pairs:
+        for _, to, of, at in pairs:
             q = query_buf[to, pl.ds(of, 1), :].astype(bf16)
             scores.append(lax.dot_general(q, keys[at], NT, preferred_element_type=f32))
             biases.append(bias_buf[to, pl.ds(of, 1), :])
@@ -237,23 +249,17 @@
         probs = jnp.where(alive, jnp.exp(logits - peak), 0.0)
         block_total = jnp.sum(probs, axis=1, keepdims=True)
         stats = jnp.where(low_half[: len(pairs)], peak, block_total)
-        for k, (owner, _, _, at, _, _) in enumerate(pairs):
+        for k, (owner, _, _, at) in enumerate(pairs):
             send2[owner, 0:1, :] = jnp.dot(
                 probs[k : k + 1].astype(bf16), values[at], preferred_element_type=f32
             )
             send2[owner, 1:2, :] = stats[k : k + 1]
-        for owner, _, _, _, dz, j in pairs:
-            send = lambda owner=owner: put(PART, send2.at[owner], recv2.at[kv], owner)
-            if dz:
-                send()
-            else:
-                pl.when(j != y)(send)
+        for owner, _, _, _ in pairs:
+            put(PART, send2.at[owner], recv2.at[kv], owner, other)
 
     part([8, 7, 9])
-    part([6, 10, 5, 11])
-    part([4, 12, 3, 13])
-    part([2, 14, 1, 15, 0])
-    recv2[kv] = send2[kv]
+    part([6, 10, 5, 11, 4, 12])
+    part([3, 13, 2, 14, 1, 15, 0])
     arrived(FAR_REST, recv_fr)
     rest_buf[...] = jnp.sum(recv_fr[...], axis=0)
     lane_1 = lax.broadcasted_iota(jnp.int32, (1, 128), 1)
@@ -261,7 +267,7 @@
     square_line = jnp.sum(recv_fsi[...], axis=0)
     square_sum = jnp.sum(jnp.where(lane_1 == my_seq, square_line, 0.0), axis=1, keepdims=True)
     my_scale = lax.rsqrt(square_sum / D + NORM_EPS)
-    query = query_buf[near, pl.ds(far, 1), :]
+    query = (rest_buf[3, pl.ds(far, 1), :] * my_scale).astype(bf16).astype(f32)
     key_new = (rest_buf[0, pl.ds(far, 1), :] * my_scale).astype(bf16).astype(f32)
     value_new = (rest_buf[1, pl.ds(far, 1), :] * my_scale).astype(bf16).astype(f32)
     gate_in = rest_buf[2, pl.ds(far, 1), :][:, 0:1] * my_scale
@@ -281,7 +287,6 @@
     attended = numerator / denominator
     send_a[...] = attended
     my_pair = near * 4 + far
-    recv_a[my_pair] = attended
     to_kv(ATT, send_a, recv_a.at[my_pair])
     loaded("wo", "gain_att", "gain_mlp", "wu", "wd")
     arrived(ATT, recv_a)
@@ -312,12 +317,10 @@
 
     mixer_in = (residual * gain_mlp_ref[...].astype(f32)).astype(bf16)
     send_sm[...] = as_row(jnp.sum(residual * residual, axis=1, keepdims=True))
-    recv_sm[near] = send_sm[...]
     to_group(SQ_MIX, lambda to: send_sm, recv_sm.at[near])
     for u in range(BLOCKS):
         part = jnp.dot(mixer_in, wu[:, u * 128 : (u + 1) * 128], preferred_element_type=f32)
         send_u[u] = part.astype(bf16)
-    recv_u[near] = send_u[near]
     to_group(UP, lambda to: send_u.at[to], recv_u.at[near])
     arrived(SQ_MIX, recv_sm)
     send_fsm[...] = jnp.sum(recv_sm[...], axis=0)
@@ -334,7 +337,6 @@
     active = jnp.maximum(jnp.sum(recv_fu[...].astype(f32), axis=0) * scale_mixer, 0.0)
     hidden = (active * active).astype(bf16)
     send_h[...] = hidden
-    recv_h[near] = hidden
     to_group(HIDDEN, lambda to: send_h, recv_h.at[near])
 
     arrived(HIDDEN, recv_h)
@@ -377,8 +379,8 @@
         V((GROUP, 4, 128), f32), V((GROUP, 4, 128), f32),
         V((GROUP, 3, 4, 128), f32), V((GROUP, 3, 4, 128), f32),
         V((1, 128), f32), V((GROUP, 1, 128), f32), V((1, 128), f32), V((FARS, 1, 128), f32),
-        V((4, 128), f32), V((NKV, 4, 128), f32), V((3, 4, 128), f32), V((FARS, 3, 4, 128), f32),
-        V((3, 4, 128), f32),
+        V((4, 128), f32), V((NKV, 4, 128), f32), V((4, 4, 128), f32), V((FARS, 4, 4, 128), f32),
+        V((4, 4, 128), f32),
         V((NKV, 2, 128), f32), V((NKV, 2, 128), f32),
         V((1, 128), f32), V((NKV, 1, 128), f32),
         V((SEQS // 2, 128), f32), V((NTP, SEQS // 2, 128), f32),
@@ -390,6 +392,7 @@
         V((SEQS // 2, 128), f32), V((NTP, SEQS // 2, 128), f32),
         pltpu.SemaphoreType.DMA((15,)),
         pltpu.SemaphoreType.DMA((EXCHANGES,)), pltpu.SemaphoreType.DMA((EXCHANGES,)),
+        pltpu.SemaphoreType.REGULAR, pltpu.SemaphoreType.REGULAR,
     ]
     return pl.pallas_call(
         kernel,

time: 76.4 us -> 73.9 us (0.967)
  Pallas kernels: 75.6 us -> 73.1 us
    pallas_call x1, Pallas kernels: 75.6 us -> 73.1 us  [per_device(): pl.pallas_call(kernel, out_shape=pltpu.VMEM((SEQS, COLS), bf16), in_specs...]
where the time goes in v4:
time: 73.9 us; the launch traced here: 73.7 us
  Pallas kernels  73.1 us (99%)
    pallas_call x1, Pallas kernels, per_device(): pl.pallas_call(kernel, out_shape=pltpu.VMEM((SEQS, COLS), bf16), in_specs...  73.1 us

profile of v4, /device:TPU:1, one launch (start us, length us, event | category | flops | bytes accessed | tf_op | source)
XLA Modules:
  0.0 73.7 jit_solution(707901393808733945)
XLA Ops:
  0.0 73.1 %shard_map.145 = bf16[32,64]{1,0:T(8,128)(2,1)S(1)} custom-call(bf16[32,64]{1,0:T(8,128)(2,1)} %stream_hbm.1, bf16[1,64]{1,0:T(2,128)(2,1)} %bitcast.9, bf16[64,256]{1,0:T(8,128)(2,1)} %wq_hbm.1, bf16[64,256]{1,0:T(8,128)(2,1)} %wk_hbm.1, bf16[64,256]{1,0:T(8,128)(2,1)} %wv_hbm.1, bf16[16,4096]{1,0:T(8,128)(2,1)} %bitcast.7, ...), custom_call_target="tpu_custom_call" | custom-call | tf_op jit(solution)/shard_map/pallas_call | solution.py:397
  73.1 0.6 copy.17

commit v5 on v4

--- a/solution.py
+++ b/solution.py
@@ -37,7 +37,7 @@
     stream_ref, gain_in_ref, wq, wk, wv, wf, keys, values, decay_ref, lengths_ref, gain_att_ref,
     wo, gain_mlp_ref, wu, wd,
     len_buf, bias_buf, query_buf,
-    send_qi, recv_qi, send_ri, recv_ri, send_si, recv_si, send_fsi, recv_fsi, send_q, recv_q, send_fr, recv_fr, rest_buf,
+    send_qi, recv_qi, send_ri, recv_ri, send_si, recv_si, send_fsi, recv_fsi, send_q, recv_q, send_fr, recv_fr,
     send2, recv2, send_a, recv_a, send_o, recv_o, send_os, recv_os,
     send_u, recv_u, send_sm, recv_sm, send_fu, recv_fu, send_fsm, recv_fsm, send_h, recv_h,
     send_d, recv_d,
@@ -210,10 +210,12 @@
     to_far(FAR_SQ_IN, lambda to: send_fsi, recv_fsi.at[far], (2,))
     to_kv(QUERY, send_q, recv_q.at[kv])
     arrived(REST_IN, recv_ri)
-    send_fr[:3] = jnp.sum(recv_ri[...], axis=0)
-    send_fr[3] = send_q[...]
-    recv_fr[far] = send_fr[...]
-    to_far(FAR_REST, lambda to: send_fr, recv_fr.at[far])
+    rest = jnp.sum(recv_ri[...], axis=0)
+    for r in range(3):
+        send_fr[:, r, :] = rest[r]
+    send_fr[:, 3, :] = send_q[...]
+    recv_fr[far] = send_fr[far]
+    to_far(FAR_REST, lambda to: send_fr.at[to], recv_fr.at[far])
     arrived(FAR_SQ_IN, recv_fsi)
     scale_in = lax.rsqrt(as_column(jnp.sum(recv_fsi[...], axis=0)) / D + NORM_EPS)
     scale_rows = jnp.broadcast_to(scale_in, (SEQS, 128)).reshape(SEQS // 4, 4, 128)
@@ -261,16 +263,16 @@
     part([6, 10, 5, 11, 4, 12])
     part([3, 13, 2, 14, 1, 15, 0])
     arrived(FAR_REST, recv_fr)
-    rest_buf[...] = jnp.sum(recv_fr[...], axis=0)
+    rest = jnp.sum(recv_fr[...], axis=0)
     lane_1 = lax.broadcasted_iota(jnp.int32, (1, 128), 1)
     my_seq = lax.rem(near, SEQS // 4) * 4 + far
     square_line = jnp.sum(recv_fsi[...], axis=0)
     square_sum = jnp.sum(jnp.where(lane_1 == my_seq, square_line, 0.0), axis=1, keepdims=True)
     my_scale = lax.rsqrt(square_sum / D + NORM_EPS)
-    query = (rest_buf[3, pl.ds(far, 1), :] * my_scale).astype(bf16).astype(f32)
-    key_new = (rest_buf[0, pl.ds(far, 1), :] * my_scale).astype(bf16).astype(f32)
-    value_new = (rest_buf[1, pl.ds(far, 1), :] * my_scale).astype(bf16).astype(f32)
-    gate_in = rest_buf[2, pl.ds(far, 1), :][:, 0:1] * my_scale
+    query = (rest[3:4, :] * my_scale).astype(bf16).astype(f32)
+    key_new = (rest[0:1, :] * my_scale).astype(bf16).astype(f32)
+    value_new = (rest[1:2, :] * my_scale).astype(bf16).astype(f32)
+    gate_in = rest[2:3, 0:1] * my_scale
     forget = jnp.minimum(gate_in, 0.0) - jnp.log1p(jnp.exp(-jnp.abs(gate_in)))
     own = jnp.sum(query * key_new, axis=1, keepdims=True) * score_scale
     arrived(PART, recv2)
@@ -379,8 +381,7 @@
         V((GROUP, 4, 128), f32), V((GROUP, 4, 128), f32),
         V((GROUP, 3, 4, 128), f32), V((GROUP, 3, 4, 128), f32),
         V((1, 128), f32), V((GROUP, 1, 128), f32), V((1, 128), f32), V((FARS, 1, 128), f32),
-        V((4, 128), f32), V((NKV, 4, 128), f32), V((4, 4, 128), f32), V((FARS, 4, 4, 128), f32),
-        V((4, 4, 128), f32),
+        V((4, 128), f32), V((NKV, 4, 128), f32), V((4, 4, 128), f32), V((FARS, 4, 128), f32),
         V((NKV, 2, 128), f32), V((NKV, 2, 128), f32),
         V((1, 128), f32), V((NKV, 1, 128), f32),
         V((SEQS // 2, 128), f32), V((NTP, SEQS // 2, 128), f32),

time: 73.9 us -> 73.2 us (level)
  no operation moved by 1% of the time
where the time goes in v5:
time: 73.2 us; the launch traced here: 73.1 us
  Pallas kernels  72.5 us (99%)
    pallas_call x1, Pallas kernels, per_device(): pl.pallas_call(kernel, out_shape=pltpu.VMEM((SEQS, COLS), bf16), in_specs...  72.5 us

profile of v5, /device:TPU:1, one launch (start us, length us, event | category | flops | bytes accessed | tf_op | source)
XLA Modules:
  0.0 73.1 jit_solution(13528485311235421020)
XLA Ops:
  0.0 72.5 %shard_map.145 = bf16[32,64]{1,0:T(8,128)(2,1)S(1)} custom-call(bf16[32,64]{1,0:T(8,128)(2,1)} %stream_hbm.1, bf16[1,64]{1,0:T(2,128)(2,1)} %bitcast.9, bf16[64,256]{1,0:T(8,128)(2,1)} %wq_hbm.1, bf16[64,256]{1,0:T(8,128)(2,1)} %wk_hbm.1, bf16[64,256]{1,0:T(8,128)(2,1)} %wv_hbm.1, bf16[16,4096]{1,0:T(8,128)(2,1)} %bitcast.7, ...), custom_call_target="tpu_custom_call" | custom-call | tf_op jit(solution)/shard_map/pallas_call | solution.py:398
  72.5 0.6 copy.17

commit v6 on v5

--- a/solution.py
+++ b/solution.py
@@ -209,13 +209,6 @@
     pl.semaphore_wait(opposite_sem, 1)
     to_far(FAR_SQ_IN, lambda to: send_fsi, recv_fsi.at[far], (2,))
     to_kv(QUERY, send_q, recv_q.at[kv])
-    arrived(REST_IN, recv_ri)
-    rest = jnp.sum(recv_ri[...], axis=0)
-    for r in range(3):
-        send_fr[:, r, :] = rest[r]
-    send_fr[:, 3, :] = send_q[...]
-    recv_fr[far] = send_fr[far]
-    to_far(FAR_REST, lambda to: send_fr.at[to], recv_fr.at[far])
     arrived(FAR_SQ_IN, recv_fsi)
     scale_in = lax.rsqrt(as_column(jnp.sum(recv_fsi[...], axis=0)) / D + NORM_EPS)
     scale_rows = jnp.broadcast_to(scale_in, (SEQS, 128)).reshape(SEQS // 4, 4, 128)
@@ -260,6 +253,13 @@
             put(PART, send2.at[owner], recv2.at[kv], owner, other)
 
     part([8, 7, 9])
+    arrived(REST_IN, recv_ri)
+    rest = jnp.sum(recv_ri[...], axis=0)
+    for r in range(3):
+        send_fr[:, r, :] = rest[r]
+    send_fr[:, 3, :] = send_q[...]
+    recv_fr[far] = send_fr[far]
+    to_far(FAR_REST, lambda to: send_fr.at[to], recv_fr.at[far])
     part([6, 10, 5, 11, 4, 12])
     part([3, 13, 2, 14, 1, 15, 0])
     arrived(FAR_REST, recv_fr)

time: 73.2 us -> 73.5 us (level)
  no operation moved by 1% of the time
where the time goes in v6:
time: 73.5 us; the launch traced here: 73.4 us
  Pallas kernels  72.8 us (99%)
    pallas_call x1, Pallas kernels, per_device(): pl.pallas_call(kernel, out_shape=pltpu.VMEM((SEQS, COLS), bf16), in_specs...  72.8 us

profile of v6, /device:TPU:1, one launch (start us, length us, event | category | flops | bytes accessed | tf_op | source)
XLA Modules:
  0.0 73.4 jit_solution(12261356479281767936)
XLA Ops:
  0.0 72.8 %shard_map.145 = bf16[32,64]{1,0:T(8,128)(2,1)S(1)} custom-call(bf16[32,64]{1,0:T(8,128)(2,1)} %stream_hbm.1, bf16[1,64]{1,0:T(2,128)(2,1)} %bitcast.9, bf16[64,256]{1,0:T(8,128)(2,1)} %wq_hbm.1, bf16[64,256]{1,0:T(8,128)(2,1)} %wk_hbm.1, bf16[64,256]{1,0:T(8,128)(2,1)} %wv_hbm.1, bf16[16,4096]{1,0:T(8,128)(2,1)} %bitcast.7, ...), custom_call_target="tpu_custom_call" | custom-call | tf_op jit(solution)/shard_map/pallas_call | solution.py:398
  72.8 0.6 copy.17
